TPU v7x, 128 devices: a whole 4x4x4 slice. The times are simulated.
128 devices in a mesh: sp: 16 (over z, y), tp: 8 (over x, core).
Axes of the slice: x: 4, y: 4, z: 4, core: 2. Of those that a mesh axis runs over, the one named last changes fastest.
Arguments:
- stream_in: bfloat16 [8192, 4096], P('sp', 'tp'), may hold values from -12 to 12
- norm_gain: float32 [2, 4096], replicated, may hold values from 0.1 to 1.9
- value_proj: bfloat16 [2, 4096, 4096], P(None, 'sp', 'tp'), may hold values from -0.09375 to 0.09375
- gate_proj: bfloat16 [2, 4096, 4096], P(None, 'sp', 'tp'), may hold values from -0.09375 to 0.09375
- out_proj: bfloat16 [2, 4096, 4096], P(None, 'sp', 'tp'), may hold values from -0.1875 to 0.1875
- conv_taps: float32 [2, 4, 4096], replicated, may hold values from -3 to 3
- block_gates: bfloat16 [2, 2, 2, 4096, 128], P(None, None, None, 'tp'), may hold values from -0.5 to 0.5
- forget_rate: float32 [2, 2, 4096], replicated, may hold values from 0 to 0.05, as said below
Outputs:
- stream_out: bfloat16 [8192, 4096], P('sp', 'tp')
Inputs may be any that keep to these rules, and one draw needn't show every extreme that they name: `forget_rate`: positive.
All inputs are finite; a program needn't handle non-finite values.
Results may differ from a plain program's by a relative error of at most 0.025.
Values may be sent and summed in bfloat16 or wider, within the bound.
A program may use at most 192 MiB of HBM per device.

v0:
```python
import jax
import jax.numpy as jnp
from jax import lax
from jax.sharding import PartitionSpec as P

GATE_SCALE = 8.0
NORM_EPS = 1e-06


def in_one_piece(arrays, axis, dim, along):
    widths = [a.shape[along] for a in arrays]
    both = jnp.concatenate(arrays, axis=along)
    out = lax.all_gather(both, axis, axis=dim, tiled=True)
    return tuple(jnp.split(out, [sum(widths[:k]) for k in range(1, len(widths))], axis=along))


def copy_for_each(array, axis):
    count = lax.axis_size(axis)
    return lax.all_to_all(
        jnp.broadcast_to(array[None], (count, *array.shape)), axis, 0, 0, tiled=True
    )


def taken_together(array, axis):
    return copy_for_each(array, axis).sum(axis=0)


def extended(cells, sides, width):
    for axis, dim in sides:
        count = lax.axis_size(axis)
        ends = count - 1
        head = lax.slice_in_dim(cells, 0, width, axis=dim)
        tail = lax.slice_in_dim(cells, cells.shape[dim] - width, cells.shape[dim], axis=dim)
        cells = jnp.concatenate(
            [
                lax.ppermute(tail, axis, [(i, (i + 1) % count) for i in range(ends)]),
                cells,
                lax.ppermute(head, axis, [((i + 1) % count, i) for i in range(ends)]),
            ],
            axis=dim,
        )
    return cells


def gathered_once(array, axis):
    leaves = jax.tree.leaves(array)
    sequence = sorted(range(len(leaves)), key=lambda k: -leaves[k].size)
    width = (1, *leaves[sequence[0]].shape)[-1]
    lines = [
        jnp.pad(leaves[k].reshape(-1), (0, -leaves[k].size % width)).reshape(-1, width)
        for k in sequence
    ]
    both, at, found = (copy_for_each(jnp.concatenate(lines), axis), 0, {})
    for k, line in zip(sequence, lines):
        slab = both[:, at : at + len(line)].reshape(len(both), -1)
        found[k] = slab[:, : leaves[k].size].reshape(-1, *leaves[k].shape)
        at += len(line)
    numbers = iter(range(len(leaves)))
    return jax.tree.map(lambda _: found[next(numbers)], array)


def folded_in_pairs(pieces, combine):
    while len(jax.tree.leaves(pieces)[0]) > 1:
        pieces = jax.vmap(combine)(
            *(jax.tree.map(lambda part: part[side::2], pieces) for side in (0, 1))
        )
    return jax.tree.map(lambda part: part[0], pieces)


def entering(array, axis, combine, identity, reverse):
    count, mine = (lax.axis_size(axis), lax.axis_index(axis))
    passed = jnp.arange(count) > mine if reverse else jnp.arange(count) < mine

    def kept(part, zero, own):
        part = jnp.where(
            passed.reshape(-1, *(1 for _ in own.shape)), part, jnp.asarray(zero, own.dtype)
        )
        return part[::-1] if reverse else part

    pieces = gathered_once(array, axis)
    return folded_in_pairs(jax.tree.map(kept, pieces, identity, array), combine)


def in_blocks(array, dim, count):
    dims = array.shape
    blocks = array.reshape(*dims[:dim], count, dims[dim] // count, *dims[dim + 1 :])
    return jnp.moveaxis(blocks, dim, 0)


def summed_on_arrival(array, axis, dim):
    blocks = in_blocks(array, dim, lax.axis_size(axis))
    arrived = lax.all_to_all(blocks, axis, split_axis=0, concat_axis=0, tiled=True)
    return arrived.astype(jnp.float32).sum(axis=0)


def pair_combine(earlier, latter):
    return (earlier[0] * latter[0], latter[0] * earlier[1] + latter[1])


def convolve(padded, taps_layer, length):
    values = padded.astype(jnp.float32)
    return sum((values[offset : offset + length] * taps_layer[offset] for offset in range(4)))


def gate_inputs(conv_out, gate_layer):
    count, width = conv_out.shape
    block_size = gate_layer.shape[-1]
    nblocks = width // block_size
    blocked = conv_out.reshape(count, nblocks, block_size)
    weights = gate_layer.astype(jnp.float32).reshape(4, nblocks, block_size, block_size)
    pre = jnp.einsum("tnc,gncd->gtnd", blocked, weights)
    return pre.reshape(4, count, width)


def decay_inputs(conv_out, pre, rate_layer, direction):
    recur_gate = jax.nn.sigmoid(pre[2 * direction])
    input_gate = jax.nn.sigmoid(pre[2 * direction + 1])
    log_decay = -GATE_SCALE * recur_gate * rate_layer[direction]
    decay = jnp.exp(log_decay)
    drive = jnp.sqrt(-jnp.expm1(2.0 * log_decay)) * input_gate * conv_out
    return (decay, drive)


def per_device(
    stream_in, norm_gain, value_proj, gate_proj, out_proj, conv_taps, block_gates, forget_rate
):
    tp_rank = lax.axis_index("tp")
    tokens_own = stream_in.shape[0]
    feat_own = stream_in.shape[1]
    width_own = value_proj.shape[2]
    ones_row = jnp.ones((width_own,), jnp.float32)
    zeros_row = jnp.zeros((width_own,), jnp.float32)
    stream = stream_in
    every_x, every_z, every_out = in_one_piece((value_proj, gate_proj, out_proj), "sp", 1, 0)
    for layer_index in range(value_proj.shape[0]):
        full_x = every_x[layer_index]
        full_z = every_z[layer_index]
        full_out = every_out[layer_index]
        values = stream.astype(jnp.float32)
        squares = taken_together(jnp.sum(values * values, axis=1), "tp")
        scale = lax.rsqrt(squares / norm_gain.shape[1] + NORM_EPS)
        gain_own = lax.dynamic_slice_in_dim(norm_gain[layer_index], tp_rank * feat_own, feat_own, 0)
        normed = (values * scale[:, None] * gain_own).astype(jnp.bfloat16)
        piece = lax.all_gather(normed, "tp", axis=1, tiled=True)
        proj_x = jnp.dot(piece, full_x, preferred_element_type=jnp.float32)
        proj_z = jnp.dot(piece, full_z, preferred_element_type=jnp.float32)
        mix_in = proj_x.astype(jnp.bfloat16)
        gate_z = proj_z.astype(jnp.bfloat16)
        padded = extended(mix_in, (("sp", 0),), 2)
        taps_own = lax.dynamic_slice_in_dim(
            conv_taps[layer_index], tp_rank * width_own, width_own, 1
        )
        rate_own = lax.dynamic_slice_in_dim(
            forget_rate[layer_index], tp_rank * width_own, width_own, 1
        )
        conv_out = convolve(padded, taps_own, tokens_own)
        pre = gate_inputs(conv_out, block_gates[layer_index])
        fwd_decay, fwd_drive = decay_inputs(conv_out, pre, rate_own, 0)
        bwd_decay, bwd_drive = decay_inputs(conv_out, pre, rate_own, 1)
        fwd_cum, fwd_state = lax.associative_scan(pair_combine, (fwd_decay, fwd_drive), axis=0)
        bwd_cum_flip, bwd_flip = lax.associative_scan(
            pair_combine, (jnp.flip(bwd_decay, 0), jnp.flip(bwd_drive, 0)), axis=0
        )
        bwd_cum = jnp.flip(bwd_cum_flip, 0)
        bwd_state = jnp.flip(bwd_flip, 0)
        enter_fwd = entering(
            (fwd_cum[-1], fwd_state[-1]), "sp", pair_combine, (ones_row, zeros_row), False
        )[1]
        enter_bwd = entering(
            (bwd_cum[0], bwd_state[0]), "sp", pair_combine, (ones_row, zeros_row), True
        )[1]
        both = fwd_state + fwd_cum * enter_fwd + bwd_state + bwd_cum * enter_bwd
        mixed = (both * jax.nn.silu(gate_z.astype(jnp.float32))).astype(jnp.bfloat16)
        partial_value = lax.dot_general(
            mixed, full_out, (((1,), (1,)), ((), ())), preferred_element_type=jnp.float32
        )
        branch = summed_on_arrival(partial_value.astype(jnp.bfloat16), "tp", 1)
        stream = (values + branch).astype(jnp.bfloat16)
    return stream


def solution(mesh):
    placed = (
        P("sp", "tp"),
        P(),
        P(None, "sp", "tp"),
        P(None, "sp", "tp"),
        P(None, "sp", "tp"),
        P(),
        P(None, None, None, "tp", None),
        P(),
    )
    return jax.shard_map(
        per_device, mesh=mesh, in_specs=placed, out_specs=P("sp", "tp"), check_vma=False
    )
```

profile of v0, /device:TPU:1, one launch (start us, length us, event | category | flops | bytes accessed | tf_op | source)
XLA Modules:
  0.0 751.1 jit_solution(18267312224000075002)
XLA Ops:
  8.5 5.8 all-to-all-start
  26.5 27.6 %all-gather.4.cloned.1.call-done = bf16[512,4096]{1,0:T(8,128)(2,1)} async-done(((bf16[512,512]{1,0:T(8,128)(2,1)}), bf16[512,4096]{1,0:T(8,128)(2,1)}) %all-gather.4.cloned.1.call-update) | async-done | bytes 4194320 | tf_op jit(solution)/shard_map/all_gather | solution.py:144
  54.1 155.8 %all-gather.6.cloned.1.call-done = bf16[6,4096,512]{2,1,0:T(8,128)(2,1)} async-done(((bf16[6,256,512]{2,1,0:T(8,128)(2,1)}), bf16[6,4096,512]{2,1,0:T(8,128)(2,1)}) %all-gather.6.cloned.1.call-update) | async-done | bytes 25165840 | tf_op jit(solution)/shard_map/all_gather | solution.py:13
  209.9 5.8 fusion.4
  234.9 5.1 multiply_multiply_fusion.3
  292.3 4.8 slice.1647
  346.4 4.6 pad.456
  358.7 8.0 %all-to-all-start.1 = ((f32[16,2,512]{2,1,0:T(2,128)}), f32[16,2,512]{2,1,0:T(2,128)S(1)}, u32[]{:S(2)}, u32[]{:S(2)}) async-start(f32[16,2,512]{2,1,0:T(2,128)} %broadcast_in_dim.88), calls=%async_computation.1 | async-start | bytes 131072 | tf_op jit(solution)/shard_map/all_to_all | solution.py:19
  366.7 5.3 rev.21
  373.9 6.4 all-to-all-start.2
  380.7 6.1 all-to-all-done.2
  387.7 7.3 fusion.12
  399.9 57.0 %all_to_all.42 = bf16[8,512,512]{2,1,0:T(8,128)(2,1)S(1)} all-to-all(bf16[8,512,512]{2,1,0:T(8,128)(2,1)S(1)} %bitcast.122), channel_id=1, replica_groups=mesh['sp'=16,'tp'=8] {'tp'}, dimensions={0} | all-to-all | bytes 8388608 | tf_op jit(solution)/shard_map/all_to_all | solution.py:92
  468.9 28.4 %all-gather.8.cloned.1.call-done = bf16[512,4096]{1,0:T(8,128)(2,1)} async-done(((bf16[512,512]{1,0:T(8,128)(2,1)}), bf16[512,4096]{1,0:T(8,128)(2,1)}) %all-gather.8.cloned.1.call-update) | async-done | bytes 4194320 | tf_op jit(solution)/shard_map/all_gather | solution.py:144
  497.2 5.8 fusion.6
  522.4 5.1 multiply_multiply_fusion.1
  579.8 4.8 slice.1886
  633.7 4.6 pad.528
  646.0 8.2 %all-to-all-start.5 = ((f32[16,2,512]{2,1,0:T(2,128)}), f32[16,2,512]{2,1,0:T(2,128)S(1)}, u32[]{:S(2)}, u32[]{:S(2)}) async-start(f32[16,2,512]{2,1,0:T(2,128)} %broadcast_in_dim.94), calls=%async_computation.5 | async-start | bytes 131072 | tf_op jit(solution)/shard_map/all_to_all | solution.py:19
  654.3 5.3 rev.23
  661.5 6.2 all-to-all-start.6
  668.1 6.1 all-to-all-done.6
  675.1 7.2 fusion.17
  687.3 55.1 %all_to_all.43 = bf16[8,512,512]{2,1,0:T(8,128)(2,1)S(1)} all-to-all(bf16[8,512,512]{2,1,0:T(8,128)(2,1)S(1)} %bitcast.123), channel_id=1, replica_groups=mesh['sp'=16,'tp'=8] {'tp'}, dimensions={0} | all-to-all | bytes 8388608 | tf_op jit(solution)/shard_map/all_to_all | solution.py:92
  (915 shorter events, 297.7 us)
Async XLA Ops:
  8.5 10.4 %all-to-all-start = ((f32[8,1,512]{2,1,0:T(1,128)}), f32[8,1,512]{2,1,0:T(1,128)S(1)}, u32[]{:S(2)}, u32[]{:S(2)}) async-start(f32[8,1,512]{2,1,0:T(1,128)} %broadcast_in_dim.86), calls=%async_computation | async-start | bytes 32768 | tf_op jit(solution)/shard_map/all_to_all | solution.py:19
  14.3 39.9 %all-gather.4.cloned.1.call-start = ((), (), s32[]{:S(2)}) async-start(), calls=%async_computation.8 | async-start | bytes 4718592 | tf_op jit(solution)/shard_map/all_gather | solution.py:144
  21.0 188.9 %all-gather.6.cloned.1.call-start = ((), (), s32[]{:S(2)}) async-start(), calls=%async_computation.9 | async-start | bytes 26738688 | tf_op jit(solution)/shard_map/all_gather | solution.py:13
  215.8 5.0 collective-permute-start
  218.9 4.3 collective-permute-start.1
  351.0 29.4 %copy-start.85 = (pred[16]{0:T(512)(128)(4,1)S(1)}, pred[16]{0:T(512)(128)(4,1)}, u32[]{:S(2)}) copy-start(pred[16]{0:T(512)(128)(4,1)} %iota_compare_fusion.1) | copy-start | bytes 52
  351.0 35.9 %copy-start.83 = (pred[16]{0:T(512)(128)(4,1)S(1)}, pred[16]{0:T(512)(128)(4,1)}, u32[]{:S(2)}) copy-start(pred[16]{0:T(512)(128)(4,1)} %iota_compare_fusion) | copy-start | bytes 52
  356.5 31.2 %copy-start.15 = (f32[512,512]{1,0:T(8,128)S(1)}, f32[512,512]{1,0:T(8,128)}, u32[]{:S(2)}) copy-start(f32[512,512]{1,0:T(8,128)} %pad.474) | copy-start | bytes 3145732
  358.7 14.6 %all-to-all-start.1 = ((f32[16,2,512]{2,1,0:T(2,128)}), f32[16,2,512]{2,1,0:T(2,128)S(1)}, u32[]{:S(2)}, u32[]{:S(2)}) async-start(f32[16,2,512]{2,1,0:T(2,128)} %broadcast_in_dim.88), calls=%async_computation.1 | async-start | bytes 131072 | tf_op jit(solution)/shard_map/all_to_all | solution.py:19
  373.9 12.9 %all-to-all-start.2 = ((f32[16,2,512]{2,1,0:T(2,128)}), f32[16,2,512]{2,1,0:T(2,128)S(1)}, u32[]{:S(2)}, u32[]{:S(2)}) async-start(f32[16,2,512]{2,1,0:T(2,128)} %broadcast_in_dim.92), calls=%async_computation.2 | async-start | bytes 131072 | tf_op jit(solution)/shard_map/all_to_all | solution.py:19
  458.2 44.9 %copy-start.5 = (bf16[512,512]{1,0:T(8,128)(2,1)}, bf16[512,512]{1,0:T(8,128)(2,1)S(1)}, u32[]{:S(2)}) copy-start(bf16[512,512]{1,0:T(8,128)(2,1)S(1)} %get-tuple-element.6) | copy-start | bytes 1572868
  458.8 9.0 %all-to-all-start.4 = ((f32[8,1,512]{2,1,0:T(1,128)}), f32[8,1,512]{2,1,0:T(1,128)S(1)}, u32[]{:S(2)}, u32[]{:S(2)}) async-start(f32[8,1,512]{2,1,0:T(1,128)} %broadcast_in_dim.93), calls=%async_computation.4 | async-start | bytes 32768 | tf_op jit(solution)/shard_map/all_to_all | solution.py:19
  463.1 34.1 %all-gather.8.cloned.1.call-start = ((), (), s32[]{:S(2)}) async-start(), calls=%async_computation.10 | async-start | bytes 4718592 | tf_op jit(solution)/shard_map/all_gather | solution.py:144
  468.8 42.0 %copy-start.33 = (f32[1,1,512]{2,1,0:T(1,128)S(1)}, f32[1,1,512]{2,1,0:T(1,128)}, u32[]{:S(2)}) copy-start(f32[1,1,512]{2,1,0:T(1,128)} %get-tuple-element.97) | copy-start | bytes 6148
  468.8 42.0 %copy-start.34 = (f32[1,1,512]{2,1,0:T(1,128)S(1)}, f32[1,1,512]{2,1,0:T(1,128)}, u32[]{:S(2)}) copy-start(f32[1,1,512]{2,1,0:T(1,128)} %get-tuple-element.98) | copy-start | bytes 6148
  468.8 42.0 %copy-start.35 = (f32[1,1,512]{2,1,0:T(1,128)S(1)}, f32[1,1,512]{2,1,0:T(1,128)}, u32[]{:S(2)}) copy-start(f32[1,1,512]{2,1,0:T(1,128)} %get-tuple-element.99) | copy-start | bytes 6148
  468.9 42.0 %copy-start.36 = (f32[1,1,512]{2,1,0:T(1,128)S(1)}, f32[1,1,512]{2,1,0:T(1,128)}, u32[]{:S(2)}) copy-start(f32[1,1,512]{2,1,0:T(1,128)} %get-tuple-element.100) | copy-start | bytes 6148
  503.0 4.6 collective-permute-start.2
  506.2 4.5 collective-permute-start.3
  638.3 29.4 %copy-start.86 = (pred[16]{0:T(512)(128)(4,1)S(1)}, pred[16]{0:T(512)(128)(4,1)}, u32[]{:S(2)}) copy-start(pred[16]{0:T(512)(128)(4,1)} %iota_compare_fusion.1) | copy-start | bytes 52
  638.4 35.9 %copy-start.84 = (pred[16]{0:T(512)(128)(4,1)S(1)}, pred[16]{0:T(512)(128)(4,1)}, u32[]{:S(2)}) copy-start(pred[16]{0:T(512)(128)(4,1)} %iota_compare_fusion) | copy-start | bytes 52
  643.8 31.2 %copy-start.14 = (f32[512,512]{1,0:T(8,128)S(1)}, f32[512,512]{1,0:T(8,128)}, u32[]{:S(2)}) copy-start(f32[512,512]{1,0:T(8,128)} %pad.546) | copy-start | bytes 3145732
  646.0 14.8 %all-to-all-start.5 = ((f32[16,2,512]{2,1,0:T(2,128)}), f32[16,2,512]{2,1,0:T(2,128)S(1)}, u32[]{:S(2)}, u32[]{:S(2)}) async-start(f32[16,2,512]{2,1,0:T(2,128)} %broadcast_in_dim.94), calls=%async_computation.5 | async-start | bytes 131072 | tf_op jit(solution)/shard_map/all_to_all | solution.py:19
  661.5 12.7 %all-to-all-start.6 = ((f32[16,2,512]{2,1,0:T(2,128)}), f32[16,2,512]{2,1,0:T(2,128)S(1)}, u32[]{:S(2)}, u32[]{:S(2)}) async-start(f32[16,2,512]{2,1,0:T(2,128)} %broadcast_in_dim.95), calls=%async_computation.6 | async-start | bytes 131072 | tf_op jit(solution)/shard_map/all_to_all | solution.py:19
  (76 other events, 560.8 us)
Sparse Core Ops, SparseCore 0:
  21.1 32.9 all-gather.3
  56.3 153.6 all-gather.5
  468.9 28.2 all-gather.7
where the time goes:
time: 761 us; the launch traced here: 751 us
  waiting for transfers between devices  238 us (31%)
  local copies, waits for them, and re-layouts  215 us (28%)
  blocking collectives  112 us (15%)
  other arithmetic  83.9 us (11%)
  starting transfers between devices  47.9 us (6%)
  matrix products  36.7 us (5%)
  between operations  17.1 us (2%)
    all_gather x1, waiting for transfers between devices, in_one_piece(): out = lax.all_gather(both, axis, axis=dim, tiled=True)  156 us
    all_to_all x2, blocking collectives, summed_on_arrival(): lax.all_to_all(blocks, axis, split_axis=0, concat_axis=0, tiled=True)  112 us
    slice x120, local copies, waits for them, and re-layouts, per_device(): lax.associative_scan(pair_combine, (fwd_decay, fwd_drive), axis=0)  78 us
    slice x132, local copies, waits for them, and re-layouts, per_device(): lax.associative_scan(pair_combine, (jnp.flip(bwd_decay, 0), jnp.flip(bwd_...  62.9 us
    all_gather x2, waiting for transfers between devices, per_device(): piece = lax.all_gather(normed, 'tp', axis=1, tiled=True)  56 us
    all_to_all x6, starting transfers between devices, copy_for_each(): lax.all_to_all(jnp.broadcast_to(array[None], (count, *array.shape)), axis...  38.9 us
    pad x64, local copies, waits for them, and re-layouts, per_device(): lax.associative_scan(pair_combine, (fwd_decay, fwd_drive), axis=0)  27 us
    add x72, other arithmetic, pair_combine(): return (earlier[0] * latter[0], latter[0] * earlier[1] + latter[1])  22.9 us
  transfers between devices with their start and end apart: 13, of which 11 were waited for; matrix products, arithmetic and copies ran while one was open for 3% of the time, Pallas kernels for 0%

commit v1 on v0

v1 whole, which is shorter than its diff:
```python
import functools

import jax
import jax.numpy as jnp
from jax import lax
from jax.experimental import pallas as pl
from jax.experimental.pallas import tpu as pltpu
from jax.sharding import PartitionSpec as P

GATE_SCALE = 8.0
NORM_EPS = 1e-06
MESH = pl.DeviceIdType.MESH
F32 = jnp.float32
BF16 = jnp.bfloat16
SEG = 8
ROWS = 64


def remote(src, dst, send_sem, recv_sem, dev):
    return pltpu.make_async_remote_copy(
        src_ref=src, dst_ref=dst, send_sem=send_sem, recv_sem=recv_sem, device_id=dev, device_id_type=MESH
    )


def greet(axis, count, me):
    barrier = pltpu.get_barrier_semaphore()
    for step in range(1, count):
        pl.semaphore_signal(barrier, inc=1, device_id={axis: lax.rem(me + step, count)}, device_id_type=MESH)
    return lambda: pl.semaphore_wait(barrier, count - 1)


def sigmoid(v):
    return 1.0 / (1.0 + jnp.exp(-v))


def drive_square(y):
    terms = [1.0, -1.0 / 2, 1.0 / 6, -1.0 / 24, 1.0 / 120, -1.0 / 720, 1.0 / 5040, -1.0 / 40320, 1.0 / 362880]
    total = jnp.full_like(y, terms[-1])
    for term in terms[-2::-1]:
        total = total * y + term
    return total * y


def in_row_steps(rows, body, size=ROWS):
    def step(k, carry):
        body(pl.ds(pl.multiple_of(k * size, size), size))
        return carry

    lax.fori_loop(0, rows // size, step, 0)


class Ring:
    def __init__(self, me, count):
        chips = count // 2
        self.chips = chips
        self.me = me
        self.x = me // 2
        self.c = lax.rem(me, 2)
        self.sib = self.x * 2 + 1 - self.c

    def at(self, step, other=False):
        core = 1 - self.c if other else self.c
        return lax.rem(self.x + step + self.chips, self.chips) * 2 + core


def gather_start(ring, own_ref, gain_ref, xg, ssg, send, recv, ssend, srecv, count):
    me = ring.me
    tokens = own_ref.shape[0]

    def fill(rows):
        v = own_ref[rows, :].astype(F32)
        xg[me, rows, :] = (v * gain_ref[...]).astype(BF16)

    in_row_steps(tokens, fill)
    half = tokens // 2
    a, b = pl.ds(0, half), pl.ds(half, half)
    right, left = ring.at(1), ring.at(-1)
    for k, (rows, dev) in enumerate(((a, right), (b, right), (b, left), (a, left))):
        part = xg.at[me, rows]
        remote(part, part, send.at[k], recv.at[k], {"tp": dev}).start()
    remote(xg.at[me], xg.at[me], send.at[6], recv.at[6], {"tp": ring.sib}).start()
    for k in range(tokens // 128):
        v = own_ref[pl.ds(k * 128, 128), :].astype(F32)
        total = jnp.sum(v * v, axis=1, keepdims=True)
        ssg[me, :, pl.ds(k * 128, 128)] = jnp.broadcast_to(total, (128, 128)).T[0:8, :]
    for step in range(1, count):
        dev = lax.rem(me + step, count)
        remote(ssg.at[me], ssg.at[me], ssend.at[dev], srecv.at[me], {"tp": dev}).start()


def gather_finish(ring, xg, ssg, send, recv, ssend, srecv, count):
    me = ring.me
    half = xg.shape[1] // 2
    a, b = pl.ds(0, half), pl.ds(half, half)
    right, left, far = ring.at(1), ring.at(-1), ring.at(2)

    def got(owner, rows, k):
        part = xg.at[owner, rows]
        remote(part, part, send.at[k], recv.at[k], {"tp": ring.sib}).wait_recv()
        return part

    def push(part, k, dev):
        remote(part, part, send.at[k], recv.at[k], {"tp": dev}).start()

    part = got(left, a, 0)
    push(part, 4, right)
    push(part, 7, ring.sib)
    part = got(right, b, 2)
    push(part, 5, left)
    push(part, 8, ring.sib)
    push(got(left, b, 1), 9, ring.sib)
    push(got(right, a, 3), 10, ring.sib)
    push(got(far, a, 4), 11, ring.sib)
    push(got(far, b, 5), 12, ring.sib)
    whole = xg.at[ring.sib]
    remote(whole, whole, send.at[6], recv.at[6], {"tp": ring.sib}).wait()
    owners = {7: (-1, a), 8: (1, b), 9: (-1, b), 10: (1, a), 11: (2, a), 12: (2, b)}
    for k, (step, rows) in owners.items():
        part = xg.at[ring.at(step, other=True), rows]
        remote(part, part, send.at[k], recv.at[k], {"tp": ring.sib}).wait()
    for k in range(6):
        part = xg.at[me, a]
        remote(part, part, send.at[k], recv.at[k], {"tp": right}).wait_send()
    for step in range(1, count):
        dev = lax.rem(me + step, count)
        remote(ssg.at[dev], ssg.at[dev], ssend.at[dev], srecv.at[dev], {"tp": dev}).wait()


def gather_kernel(count, own_ref, gain_ref, xg, ssg, send, recv, ssend, srecv):
    me = lax.axis_index("tp")
    ring = Ring(me, count)
    greet("tp", count, me)()
    gather_start(ring, own_ref, gain_ref, xg, ssg, send, recv, ssend, srecv, count)
    gather_finish(ring, xg, ssg, send, recv, ssend, srecv, count)


GATHER_SEMS = 13


def gather_call(own, gain, count, ident):
    tokens, feats = own.shape
    vmem = pl.BlockSpec(memory_space=pltpu.VMEM)
    return pl.pallas_call(
        functools.partial(gather_kernel, count),
        out_shape=(
            jax.ShapeDtypeStruct((count, tokens, feats), BF16),
            jax.ShapeDtypeStruct((count, 8, tokens), F32),
        ),
        in_specs=[vmem, vmem],
        out_specs=(vmem, vmem),
        scratch_shapes=[
            pltpu.SemaphoreType.DMA((GATHER_SEMS,)),
            pltpu.SemaphoreType.DMA((GATHER_SEMS,)),
            pltpu.SemaphoreType.DMA((count,)),
            pltpu.SemaphoreType.DMA((count,)),
        ],
        compiler_params=pltpu.CompilerParams(collective_id=ident, has_side_effects=True),
        cost_estimate=pl.CostEstimate(flops=20_000_000_000, bytes_accessed=8_000_000, transcendentals=0),
        name="tp_gather",
    )(own, gain)


def mix_kernel(
    count, features, xg_hbm, ssg, w_hbm, taps, rate, gates, out,
    xv, wv, acc_v, acc_g, mixb, mpad, sil, conv, convb, pre, a_f, u_f, a_b, u_b, col,
    halo_p, halo_n, seg, ent, msg, slots, ld, hsend, hrecv, csend, crecv,
):
    me = lax.axis_index("sp")
    tokens, width = mixb.shape
    blocks = xv.shape[0]
    depth = xv.shape[2]
    joined = greet("sp", count, me)

    def loads(p):
        rows = pl.ds(pl.multiple_of(p * depth, depth), depth)
        return (
            pltpu.make_async_copy(xg_hbm.at[p], xv.at[p], ld.at[0, p]),
            pltpu.make_async_copy(w_hbm.at[0, rows], wv.at[0, p], ld.at[1, p]),
            pltpu.make_async_copy(w_hbm.at[1, rows], wv.at[1, p], ld.at[2, p]),
        )

    for p in range(blocks):
        for copy in loads(p):
            copy.start()
    total = jnp.sum(ssg[...], axis=0)
    scale = lax.rsqrt(total / features + NORM_EPS)
    for k in range(tokens // 128):
        part = jnp.broadcast_to(scale[0:1, k * 128 : (k + 1) * 128], (128, 128))
        col[pl.ds(k * 128, 128), :] = part.T

    for p in range(blocks):
        for copy in loads(p):
            copy.wait()
        for side, acc in ((0, acc_v), (1, acc_g)):
            term = jnp.dot(xv[p], wv[side, p], preferred_element_type=F32)
            acc[...] = term if p == 0 else acc[...] + term

    def finish_v(rows):
        wide = jnp.concatenate([col[rows, :]] * (width // 128), axis=1)
        mix = (acc_v[rows, :] * wide).astype(BF16)
        mixb[rows, :] = mix
        acc_v[rows, :] = mix.astype(F32)

    in_row_steps(tokens, finish_v, 32)
    joined()
    head, tail = mixb.at[pl.ds(0, 16)], mixb.at[pl.ds(tokens - 16, 16)]
    to_next = remote(tail, halo_p, hsend.at[0], hrecv.at[0], {"sp": lax.rem(me + 1, count)})
    to_prev = remote(head, halo_n, hsend.at[1], hrecv.at[1], {"sp": lax.rem(me + count - 1, count)})
    to_next.start()
    to_prev.start()

    def finish_g(rows):
        wide = jnp.concatenate([col[rows, :]] * (width // 128), axis=1)
        gate = (acc_g[rows, :] * wide).astype(BF16).astype(F32)
        sil[rows, :] = gate * sigmoid(gate)
        mpad[pl.ds(pl.multiple_of(rows.start + 16, 16), rows.size), :] = acc_v[rows, :]

    in_row_steps(tokens, finish_g, 32)
    to_next.wait()
    to_prev.wait()
    sub = lax.broadcasted_iota(jnp.int32, (SEG, width), 0)
    before = halo_p[...].astype(F32)
    after = halo_n[...].astype(F32)
    for k in range(2):
        edge = jnp.where(me > 0, before[8 * k + 7 : 8 * k + 8, :], 0.0)
        blk = acc_v[pl.ds(tokens - 16 + 8 * k, 8), :]
        mpad[pl.ds(8 * k, 8), :] = jnp.where(sub == 0, jnp.broadcast_to(edge, (SEG, width)), pltpu.roll(blk, 1, 0))
    edge = jnp.where(me < count - 1, after[0:1, :], 0.0)
    blk = acc_v[pl.ds(0, 8), :]
    mpad[pl.ds(tokens + 16, 8), :] = jnp.where(
        sub == SEG - 1, jnp.broadcast_to(edge, (SEG, width)), pltpu.roll(blk, SEG - 1, 0)
    )

    def convolve(rows):
        parts = [
            mpad[pl.ds(pl.multiple_of(rows.start + 8 * k, 8), rows.size), :] * taps[k : k + 1, :] for k in range(4)
        ]
        value = (parts[0] + parts[1]) + (parts[2] + parts[3])
        conv[rows, :] = value
        convb[rows, :] = value.astype(BF16)

    in_row_steps(tokens, convolve, 32)
    for b in range(width // 128):
        pre[b] = jnp.dot(convb[:, b * 128 : (b + 1) * 128], gates[b], preferred_element_type=F32)

    for b in range(width // 128):
        lanes = pl.ds(b * 128, 128)
        rates = [-GATE_SCALE * rate[e : e + 1, lanes] for e in range(2)]

        def body(k, carry, b=b, lanes=lanes, rates=rates):
            p_f, h_f, p_b, h_b = carry
            rows = pl.ds(pl.multiple_of(k * ROWS, ROWS), ROWS)
            cv = conv[rows, lanes]
            kept = []
            for e, (a_ref, u_ref) in enumerate(((a_f, u_f), (a_b, u_b))):
                r = sigmoid(pre[b, rows, 256 * e : 256 * e + 128])
                i = sigmoid(pre[b, rows, 256 * e + 128 : 256 * e + 256])
                log_a = rates[e] * r
                decay = jnp.exp(log_a)
                drive = jnp.sqrt(drive_square(-2.0 * log_a)) * i * cv
                a_ref[rows, lanes] = decay
                u_ref[rows, lanes] = drive
                kept.append((decay, drive))
            for j in range(ROWS // 8):
                at = slice(8 * j, 8 * j + 8)
                d, u = kept[0][0][at], kept[0][1][at]
                h_f = d * h_f + u
                p_f = p_f * d
                d, u = kept[1][0][at], kept[1][1][at]
                h_b = h_b + p_b * u
                p_b = p_b * d
            return p_f, h_f, p_b, h_b

        one, zero = jnp.ones((SEG, 128), F32), jnp.zeros((SEG, 128), F32)
        done = lax.fori_loop(0, tokens // ROWS, body, (one, zero, one, zero))
        for k in range(4):
            seg[k, :, lanes] = done[k]

    sides = ((0, range(SEG)), (2, range(SEG - 1, -1, -1)))
    for e, (k, order) in enumerate(sides):
        prod = jnp.ones((1, width), F32)
        state = jnp.zeros((1, width), F32)
        for s in order:
            d = seg[k, s : s + 1, :]
            state = d * state + seg[k + 1, s : s + 1, :]
            prod = prod * d
        for b in range(width // 128):
            msg[e, b : b + 1, :] = prod[:, b * 128 : (b + 1) * 128]
            msg[e, 4 + b : 5 + b, :] = state[:, b * 128 : (b + 1) * 128]
    for step in range(1, count):
        dev = lax.rem(me + step, count)
        side = jnp.where(dev > me, 0, 1)
        remote(msg.at[side], slots.at[me], csend.at[dev], crecv.at[me], {"sp": dev}).start()
    slots[me] = jnp.zeros((8, 128), F32)
    for step in range(1, count):
        dev = lax.rem(me + step, count)
        remote(msg.at[0], slots.at[dev], csend.at[dev], crecv.at[dev], {"sp": dev}).wait()
    for e, (k, order) in enumerate(sides):
        carry = jnp.zeros((4, 128), F32)
        for q in range(count) if e == 0 else range(count - 1, -1, -1):
            live = (q < me) if e == 0 else (q > me)
            slot = slots[q]
            carry = jnp.where(live, slot[0:4] * carry + slot[4:8], carry)
        state = jnp.concatenate([carry[b : b + 1, :] for b in range(width // 128)], axis=1)
        for s in order:
            ent[e, s : s + 1, :] = state
            state = seg[k, s : s + 1, :] * state + seg[k + 1, s : s + 1, :]

    steps = tokens // SEG

    def again(k, carry):
        h_f, h_b = carry
        for j in range(4):
            fwd = pl.ds(pl.multiple_of((4 * k + j) * SEG, SEG), SEG)
            bwd = pl.ds(pl.multiple_of((steps - 1 - 4 * k - j) * SEG, SEG), SEG)
            h_f = a_f[fwd, :] * h_f + u_f[fwd, :]
            u_f[fwd, :] = h_f
            h_b = a_b[bwd, :] * h_b + u_b[bwd, :]
            u_b[bwd, :] = h_b
        return h_f, h_b

    lax.fori_loop(0, steps // 4, again, (ent[0], ent[1]))

    def gated(rows):
        out[rows, :] = ((u_f[rows, :] + u_b[rows, :]) * sil[rows, :]).astype(BF16)

    in_row_steps(tokens, gated, 32)


def mix_call(xg, ssg, weights, taps, rate, gates, count, ident):
    blocks, tokens, depth = xg.shape
    width = weights.shape[2]
    vmem = pl.BlockSpec(memory_space=pltpu.VMEM)
    hbm = pl.BlockSpec(memory_space=pl.ANY)
    full = pltpu.VMEM((tokens, width), F32)
    half = pltpu.VMEM((tokens, width), BF16)
    return pl.pallas_call(
        functools.partial(mix_kernel, count, float(blocks * depth)),
        out_shape=jax.ShapeDtypeStruct((tokens, width), BF16),
        in_specs=[hbm, vmem, hbm, vmem, vmem, vmem],
        out_specs=vmem,
        scratch_shapes=[
            pltpu.VMEM((blocks, tokens, depth), BF16),
            pltpu.VMEM((2, blocks, depth, width), BF16),
            full, full, half,
            pltpu.VMEM((tokens + 24, width), F32),
            full, full, half,
            pltpu.VMEM((width // 128, tokens, 512), F32),
            full, full, full, full,
            pltpu.VMEM((tokens, 128), F32),
            pltpu.VMEM((16, width), BF16),
            pltpu.VMEM((16, width), BF16),
            pltpu.VMEM((4, SEG, width), F32),
            pltpu.VMEM((2, SEG, width), F32),
            pltpu.VMEM((2, 8, 128), F32),
            pltpu.VMEM((count, 8, 128), F32),
            pltpu.SemaphoreType.DMA((3, blocks)),
            pltpu.SemaphoreType.DMA((2,)),
            pltpu.SemaphoreType.DMA((2,)),
            pltpu.SemaphoreType.DMA((count,)),
            pltpu.SemaphoreType.DMA((count,)),
        ],
        compiler_params=pltpu.CompilerParams(collective_id=ident, has_side_effects=True),
        cost_estimate=pl.CostEstimate(flops=20_000_000_000, bytes_accessed=14_000_000, transcendentals=0),
        name="mix",
    )(xg, ssg, weights, taps, rate, gates)


def reduce_kernel(count, mixed, w_hbm, own, out, wv, psend, precv, pown, fbuf, far_in, nbuf, near_in, ld, ds, dr, rs, rr):
    me = lax.axis_index("tp")
    ring = Ring(me, count)
    tokens, feats = own.shape
    half = tokens // 2
    a, b = pl.ds(0, half), pl.ds(half, half)
    right, left = ring.at(1), ring.at(-1)
    joined = greet("tp", count, me)
    order = (2, 1, -1, 0)

    def load(k, other):
        block = ring.at(order[k], other=other)
        rows = pl.ds(pl.multiple_of(block * feats, feats), feats)
        return pltpu.make_async_copy(w_hbm.at[rows], wv.at[2 * k + 1 - int(other)], ld.at[2 * k + 1 - int(other)])

    for k in range(4):
        load(k, True).start()
        load(k, False).start()
    joined()

    def product(k, other):
        load(k, other).wait()
        return lax.dot_general(
            mixed[...], wv[2 * k + 1 - int(other)], (((1,), (1,)), ((), ())), preferred_element_type=F32
        )

    def across(k):
        return remote(psend.at[k], precv.at[k], ds.at[k], dr.at[k], {"tp": ring.sib})

    def send(k, src, dst, dev):
        copy = remote(src, dst, rs.at[k], rr.at[k], {"tp": dev})
        copy.start()
        return copy

    def paired(k, rows, into=None):
        def body(r):
            at = pl.ds(pl.multiple_of(rows.start + r.start, 32), r.size)
            value = pown[k, at, :] + precv[k, at, :].astype(F32)
            if into is None:
                pown[k, at, :] = value
            else:
                into[at if into.shape[0] == tokens else r, :] = value.astype(BF16)

        in_row_steps(rows.size, body, 32)

    for k in range(4):
        psend[k] = product(k, True).astype(BF16)
        across(k).start()
        pown[k] = product(k, False)
        if k == 1:
            across(0).wait_recv()
            paired(0, a, fbuf)
            send(0, fbuf.at[a], far_in.at[0], right)
            paired(0, b, fbuf)
            send(1, fbuf.at[b], far_in.at[1], left)
        if k == 2:
            across(1).wait_recv()
            paired(1, b, nbuf.at[0])
            send(2, nbuf.at[0], near_in.at[0], right)
            paired(1, a)
        if k == 3:
            across(2).wait_recv()
            paired(2, a, nbuf.at[1])
            send(3, nbuf.at[1], near_in.at[1], left)
            paired(2, b)
    across(3).wait_recv()
    paired(3, pl.ds(0, tokens))

    def arrived(k, src, dst):
        remote(src, dst, rs.at[k], rr.at[k], {"tp": right}).wait_recv()

    def merged(k, rows, src, into):
        def body(r):
            at = pl.ds(pl.multiple_of(rows.start + r.start, 32), r.size)
            into[r, :] = (pown[k, at, :] + src[r, :].astype(F32)).astype(BF16)

        in_row_steps(half, body, 32)

    arrived(0, fbuf.at[a], far_in.at[0])
    merged(1, a, far_in.at[0], nbuf.at[2])
    send(4, nbuf.at[2], near_in.at[2], right)
    arrived(1, fbuf.at[b], far_in.at[1])
    merged(2, b, far_in.at[1], nbuf.at[3])
    send(5, nbuf.at[3], near_in.at[3], left)
    for k in range(4):
        arrived(2 + k, nbuf.at[k], near_in.at[k])

    def total(rows, one, two):
        def body(r):
            at = pl.ds(pl.multiple_of(rows.start + r.start, 32), r.size)
            branch = pown[3, at, :] + near_in[one, r, :].astype(F32) + near_in[two, r, :].astype(F32)
            out[at, :] = (own[at, :].astype(F32) + branch).astype(BF16)

        in_row_steps(half, body, 32)

    total(a, 1, 2)
    total(b, 0, 3)
    for k in range(4):
        across(k).wait_send()
    for k in range(6):
        remote(nbuf.at[0], near_in.at[0], rs.at[k], rr.at[k], {"tp": right}).wait_send()


def reduce_call(mixed, weights, own, count, ident):
    tokens, width = mixed.shape
    feats = own.shape[1]
    vmem = pl.BlockSpec(memory_space=pltpu.VMEM)
    hbm = pl.BlockSpec(memory_space=pl.ANY)
    half = tokens // 2
    return pl.pallas_call(
        functools.partial(reduce_kernel, count),
        out_shape=jax.ShapeDtypeStruct((tokens, feats), BF16),
        in_specs=[vmem, hbm, vmem],
        out_specs=vmem,
        scratch_shapes=[
            pltpu.VMEM((count, feats, width), BF16),
            pltpu.VMEM((4, tokens, feats), BF16),
            pltpu.VMEM((4, tokens, feats), BF16),
            pltpu.VMEM((4, tokens, feats), F32),
            pltpu.VMEM((tokens, feats), BF16),
            pltpu.VMEM((2, half, feats), BF16),
            pltpu.VMEM((4, half, feats), BF16),
            pltpu.VMEM((4, half, feats), BF16),
            pltpu.SemaphoreType.DMA((count,)),
            pltpu.SemaphoreType.DMA((4,)),
            pltpu.SemaphoreType.DMA((4,)),
            pltpu.SemaphoreType.DMA((6,)),
            pltpu.SemaphoreType.DMA((6,)),
        ],
        compiler_params=pltpu.CompilerParams(collective_id=ident, has_side_effects=True),
        cost_estimate=pl.CostEstimate(flops=20_000_000_000, bytes_accessed=8_000_000, transcendentals=0),
        name="tp_reduce",
    )(mixed, weights, own)


def per_device(
    n_sp, n_tp, stream_in, norm_gain, value_proj, gate_proj, out_proj, conv_taps, block_gates, forget_rate
):
    tp_rank = lax.axis_index("tp")
    tokens, feats = stream_in.shape
    width = value_proj.shape[2]
    layers = value_proj.shape[0]
    steps = tokens // SEG

    def gathered(array, dim):
        return lax.all_gather(array, "sp", axis=dim, tiled=True)

    def own_part(array, size):
        return lax.dynamic_slice_in_dim(array, tp_rank * size, size, array.ndim - 1)

    weights = []
    for layer in range(layers):
        pair = jnp.stack([value_proj[layer], gate_proj[layer]])
        weights.append((gathered(pair, 1), gathered(out_proj[layer], 0)))
    gain = own_part(norm_gain, feats)
    taps = own_part(conv_taps, width)
    rate = own_part(forget_rate, width)
    blocks = width // 128
    gates = block_gates.reshape(layers, 4, blocks, 128, 128).transpose(0, 2, 3, 1, 4).reshape(layers, blocks, 128, 512)
    stream = stream_in.reshape(SEG, steps, feats).transpose(1, 0, 2).reshape(tokens, feats)
    for layer in range(layers):
        both, out_w = weights[layer]
        xg, ssg = gather_call(stream, gain[layer : layer + 1], n_tp, 3 * layer)
        mixed = mix_call(xg, ssg, both, taps[layer], rate[layer], gates[layer], n_sp, 3 * layer + 1)
        stream = reduce_call(mixed, out_w, stream, n_tp, 3 * layer + 2)
    return stream.reshape(steps, SEG, feats).transpose(1, 0, 2).reshape(tokens, feats)


def solution(mesh):
    placed = (
        P("sp", "tp"),
        P(),
        P(None, "sp", "tp"),
        P(None, "sp", "tp"),
        P(None, "sp", "tp"),
        P(),
        P(None, None, None, "tp", None),
        P(),
    )
    body = functools.partial(per_device, mesh.shape["sp"], mesh.shape["tp"])
    return jax.shard_map(body, mesh=mesh, in_specs=placed, out_specs=P("sp", "tp"), check_vma=False)
```

time: 761 us -> 299 us (0.39); the launches traced: 751 us -> 298 us
  local copies, waits for them, and re-layouts: 215 us -> 13.6 us
  Pallas kernels: 0 us -> 157 us
  waiting for transfers between devices: 238 us -> 113 us
  blocking collectives: 112 us -> 0 us
  other arithmetic: 83.9 us -> 1.75 us
  starting transfers between devices: 47.9 us -> 0.13 us
  matrix products: 36.7 us -> 0 us
    pallas_call x0 -> x6, Pallas kernels: none -> 157 us  [the longest x2 58.2 us: gather_call(): pl.pallas_call(functools.partial(gather_kernel, count), out_shape=(jax.Sh...]
    slice x319 -> x4, local copies, waits for them, and re-layouts: 146 us -> 5.04 us  [the longest x1 1.87 us: per_device(): weights.append((gathered(pair, 1), gathered(out_proj[layer], 0)))]
    all_to_all x2 -> x0, blocking collectives: 112 us -> none  [summed_on_arrival(): lax.all_to_all(blocks, axis, split_axis=0, concat_axis=0, tiled=True)]
    all_gather x3 -> x4, waiting for transfers between devices: 212 us -> 112 us  [gathered(): return lax.all_gather(array, 'sp', axis=dim, tiled=True)]
    add x150 -> x0, other arithmetic: 40.6 us -> none  [the longest x72 22.9 us: pair_combine(): return (earlier[0] * latter[0], latter[0] * earlier[1] + latter[1])]
    all_to_all x6 -> x0, starting transfers between devices: 38.9 us -> none  [copy_for_each(): lax.all_to_all(jnp.broadcast_to(array[None], (count, *array.shape)), axis...]
    dot_general x8 -> x0, matrix products: 36.7 us -> none  [the longest x2 14.5 us: per_device(): proj_z = jnp.dot(piece, full_z, preferred_element_type=jnp.float32)]
    pad x128 -> x0, local copies, waits for them, and re-layouts: 33.5 us -> none  [the longest x64 27 us: per_device(): lax.associative_scan(pair_combine, (fwd_decay, fwd_drive), axis=0)]
  transfers between devices with their start and end apart: 13 -> 4, of which waited for: 11 -> 4; matrix products, arithmetic and copies ran while one was open for 3% -> 4% of each run, Pallas kernels for 0% -> 44%
where the time goes in v1:
time: 299 us; the launch traced here: 298 us
  Pallas kernels  157 us (53%)
  waiting for transfers between devices  113 us (38%)
  local copies, waits for them, and re-layouts  13.6 us (5%)
  between operations  13.2 us (4%)
    all_gather x4, waiting for transfers between devices, gathered(): return lax.all_gather(array, 'sp', axis=dim, tiled=True)  112 us
    pallas_call x2, Pallas kernels, gather_call(): pl.pallas_call(functools.partial(gather_kernel, count), out_shape=(jax.Sh...  58.2 us
    pallas_call x2, Pallas kernels, reduce_call(): pl.pallas_call(functools.partial(reduce_kernel, count), out_shape=jax.Sha...  54.2 us
    pallas_call x2, Pallas kernels, mix_call(): pl.pallas_call(functools.partial(mix_kernel, count, float(blocks * depth)...  44.8 us
  transfers between devices with their start and end apart: 4, of which 4 were waited for; matrix products, arithmetic and copies ran while one was open for 4% of the time, Pallas kernels for 44%

profile of v1, /device:TPU:1, one launch (start us, length us, event | category | flops | bytes accessed | tf_op | source)
XLA Modules:
  0.0 298.5 jit_solution(9153191720633769391)
XLA Ops:
  6.5 1.4 fusion.2
  7.9 0.8 pad_maximum_fusion
  8.8 1.9 fusion.1
  10.8 0.9 pad_maximum_fusion.1
  11.8 0.5 all-gather.13.cloned.1.call-update
  12.3 1.1 copy.15
  13.4 0.8 copy.14
  14.2 1.4 fusion.4
  15.6 29.8 %tp_gather.2 = (bf16[8,512,512]{2,1,0:T(8,128)(2,1)}, f32[8,8,512]{2,1,0:T(8,128)}) custom-call(bf16[512,512]{1,0:T(8,128)(2,1)} %bitcast.27, f32[1,512]{1,0:T(1,128)} %get-tuple-element.26.gain_ref), custom_call_target="tpu_custom_call" | custom-call | flops 20000000000 | bytes 8000000 | tf_op jit(solution)/shard_map/tp_gather/pallas_call | solution.py:143
  45.5 0.4 fusion
  45.9 1.0 squeeze.26.gates
  46.9 1.0 squeeze.30.gates
  47.9 1.3 dynamic-slice_bitcast_fusion.2
  49.2 1.3 dynamic-slice_bitcast_fusion
  50.5 33.0 %all-gather.7.cloned.1.call-done.w_hbm = bf16[2,4096,512]{2,1,0:T(8,128)(2,1)} async-done(((bf16[2,256,512]{2,1,0:T(8,128)(2,1)}), bf16[2,4096,512]{2,1,0:T(8,128)(2,1)}) %all-gather.7.cloned.1.call-update) | async-done | bytes 8388624 | tf_op jit(solution)/shard_map/all_gather | solution.py:514
  83.5 22.3 %mix.2.mixed = bf16[512,512]{1,0:T(8,128)(2,1)} custom-call(bf16[8,512,512]{2,1,0:T(8,128)(2,1)} %get-tuple-element.9.xg_hbm, f32[8,8,512]{2,1,0:T(8,128)} %get-tuple-element.10.ssg, bf16[2,4096,512]{2,1,0:T(8,128)(2,1)} %all-gather.7.cloned.1.call-done.w_hbm, f32[4,512]{1,0:T(4,128)} %get-tuple-element.22.taps, f32[2,512]{1,0:T(2,128)} %get-tuple-element.24.rate, ...), custom_call_target="tpu_custom_call" | custom-call | flops 20000000000 | bytes 14000000 | tf_op jit(solution)/shard_map/mix/pallas_call | solution.py:337
  105.8 31.2 %all-gather.11.cloned.1.call-done = bf16[1,4096,512]{2,1,0:T(8,128)(2,1)} async-done(((bf16[1,256,512]{2,1,0:T(8,128)(2,1)}), bf16[1,4096,512]{2,1,0:T(8,128)(2,1)}) %all-gather.11.cloned.1.call-update) | async-done | bytes 4194320 | tf_op jit(solution)/shard_map/all_gather | solution.py:514
  136.9 27.2 %tp_reduce.2.own_ref.own = bf16[512,512]{1,0:T(8,128)(2,1)} custom-call(bf16[512,512]{1,0:T(8,128)(2,1)} %mix.2.mixed, bf16[4096,512]{1,0:T(8,128)(2,1)} %bitcast.31, bf16[512,512]{1,0:T(8,128)(2,1)} %bitcast.28), custom_call_target="tpu_custom_call" | custom-call | flops 20000000000 | bytes 8000000 | tf_op jit(solution)/shard_map/tp_reduce/pallas_call | solution.py:478
  164.1 28.4 %tp_gather.3 = (bf16[8,512,512]{2,1,0:T(8,128)(2,1)}, f32[8,8,512]{2,1,0:T(8,128)}) custom-call(bf16[512,512]{1,0:T(8,128)(2,1)} %tp_reduce.2.own_ref.own, f32[1,512]{1,0:T(1,128)} %get-tuple-element.25.gain_ref), custom_call_target="tpu_custom_call" | custom-call | flops 20000000000 | bytes 8000000 | tf_op jit(solution)/shard_map/tp_gather/pallas_call | solution.py:143
  192.5 17.2 %all-gather.9.cloned.1.call-done.w_hbm = bf16[2,4096,512]{2,1,0:T(8,128)(2,1)} async-done(((bf16[2,256,512]{2,1,0:T(8,128)(2,1)}), bf16[2,4096,512]{2,1,0:T(8,128)(2,1)}) %all-gather.9.cloned.1.call-update) | async-done | bytes 8388624 | tf_op jit(solution)/shard_map/all_gather | solution.py:514
  209.6 22.5 %mix.3.mixed = bf16[512,512]{1,0:T(8,128)(2,1)} custom-call(bf16[8,512,512]{2,1,0:T(8,128)(2,1)} %get-tuple-element.11.xg_hbm, f32[8,8,512]{2,1,0:T(8,128)} %get-tuple-element.12.ssg, bf16[2,4096,512]{2,1,0:T(8,128)(2,1)} %all-gather.9.cloned.1.call-done.w_hbm, f32[4,512]{1,0:T(4,128)} %get-tuple-element.21.taps, f32[2,512]{1,0:T(2,128)} %get-tuple-element.23.rate, ...), custom_call_target="tpu_custom_call" | custom-call | flops 20000000000 | bytes 14000000 | tf_op jit(solution)/shard_map/mix/pallas_call | solution.py:337
  232.1 30.8 %all-gather.13.cloned.1.call-done = bf16[1,4096,512]{2,1,0:T(8,128)(2,1)} async-done(((bf16[1,256,512]{2,1,0:T(8,128)(2,1)}), bf16[1,4096,512]{2,1,0:T(8,128)(2,1)}) %all-gather.13.cloned.1.call-update) | async-done | bytes 4194320 | tf_op jit(solution)/shard_map/all_gather | solution.py:514
  262.9 27.0 %tp_reduce.3 = bf16[512,512]{1,0:T(8,128)(2,1)} custom-call(bf16[512,512]{1,0:T(8,128)(2,1)} %mix.3.mixed, bf16[4096,512]{1,0:T(8,128)(2,1)} %bitcast.30, bf16[512,512]{1,0:T(8,128)(2,1)} %tp_reduce.2.own_ref.own), custom_call_target="tpu_custom_call" | custom-call | flops 20000000000 | bytes 8000000 | tf_op jit(solution)/shard_map/tp_reduce/pallas_call | solution.py:478
  290.0 2.0 copy.11
  (11 shorter events, 0.2 us)
Async XLA Ops:
  6.5 5.8 %copy-start.1 = (bf16[512,512]{1,0:T(8,128)(2,1)S(1)}, bf16[512,512]{1,0:T(8,128)(2,1)}, u32[]{:S(2)}) copy-start(bf16[512,512]{1,0:T(8,128)(2,1)} %param.8) | copy-start | bytes 1572868
  6.5 6.9 %copy-start = (bf16[2,2,2,512,128]{4,3,2,1,0:T(8,128)(2,1)S(1)}, bf16[2,2,2,512,128]{4,3,2,1,0:T(8,128)(2,1)}, u32[]{:S(2)}) copy-start(bf16[2,2,2,512,128]{4,3,2,1,0:T(8,128)(2,1)} %param.14) | copy-start | bytes 3145732
  6.5 77.0 %all-gather.7.cloned.1.call-start = ((), (), s32[]{:S(2)}) async-start(), calls=%async_computation | async-start | bytes 8912896 | tf_op jit(solution)/shard_map/all_gather | solution.py:514
  8.8 128.1 %all-gather.11.cloned.1.call-start = ((), (), s32[]{:S(2)}) async-start(), calls=%async_computation.2 | async-start | bytes 4456448 | tf_op jit(solution)/shard_map/all_gather | solution.py:514
  10.7 198.9 %all-gather.9.cloned.1.call-start = ((), (), s32[]{:S(2)}) async-start(), calls=%async_computation.1 | async-start | bytes 8912896 | tf_op jit(solution)/shard_map/all_gather | solution.py:514
  11.7 251.2 %all-gather.13.cloned.1.call-start = ((), (), s32[]{:S(2)}) async-start(), calls=%async_computation.3 | async-start | bytes 4456448 | tf_op jit(solution)/shard_map/all_gather | solution.py:514
Sparse Core Ops, SparseCore 0:
  9.5 73.9 all-gather.6
  85.6 51.2 all-gather.10
  139.1 70.5 all-gather.8
  211.6 51.2 all-gather.12

commit v2 on v0

v2 whole, which is shorter than its diff:
```python
import functools

import jax
import jax.numpy as jnp
from jax import lax
from jax.experimental import pallas as pl
from jax.experimental.pallas import tpu as pltpu
from jax.sharding import PartitionSpec as P

GATE_SCALE = 8.0
NORM_EPS = 1e-06
MESH = pl.DeviceIdType.MESH
F32 = jnp.float32
BF16 = jnp.bfloat16
SEG = 8
ROWS = 64


def remote(src, dst, send_sem, recv_sem, dev):
    return pltpu.make_async_remote_copy(
        src_ref=src, dst_ref=dst, send_sem=send_sem, recv_sem=recv_sem, device_id=dev, device_id_type=MESH
    )


def greet(groups):
    barrier = pltpu.get_barrier_semaphore()
    for axis, count, me in groups:
        for step in range(1, count):
            pl.semaphore_signal(barrier, inc=1, device_id={axis: lax.rem(me + step, count)}, device_id_type=MESH)
    pl.semaphore_wait(barrier, sum(count - 1 for _, count, _ in groups))


def sigmoid(v):
    return 1.0 / (1.0 + jnp.exp(-v))


def drive_square(y):
    terms = [1.0, -1.0 / 2, 1.0 / 6, -1.0 / 24, 1.0 / 120, -1.0 / 720, 1.0 / 5040, -1.0 / 40320, 1.0 / 362880]
    total = jnp.full_like(y, terms[-1])
    for term in terms[-2::-1]:
        total = total * y + term
    return total * y


def in_row_steps(rows, body, size=ROWS):
    def step(k, carry):
        body(pl.ds(pl.multiple_of(k * size, size), size))
        return carry

    lax.fori_loop(0, rows // size, step, 0)


class Ring:
    def __init__(self, me, count):
        chips = count // 2
        self.chips = chips
        self.me = me
        self.x = me // 2
        self.c = lax.rem(me, 2)
        self.sib = self.x * 2 + 1 - self.c

    def at(self, step, other=False):
        core = 1 - self.c if other else self.c
        return lax.rem(self.x + step + self.chips, self.chips) * 2 + core


def gather_start(ring, own_ref, gain, xg, ssg, send, recv, ssend, srecv, count):
    me = ring.me
    tokens = own_ref.shape[0]

    def fill(rows):
        v = own_ref[rows, :].astype(F32)
        xg[me, rows, :] = (v * gain).astype(BF16)

    in_row_steps(tokens, fill)
    half = tokens // 2
    a, b = pl.ds(0, half), pl.ds(half, half)
    right, left = ring.at(1), ring.at(-1)
    for k, (rows, dev) in enumerate(((a, right), (b, right), (b, left), (a, left))):
        part = xg.at[me, rows]
        remote(part, part, send.at[k], recv.at[k], {"tp": dev}).start()
    remote(xg.at[me], xg.at[me], send.at[6], recv.at[6], {"tp": ring.sib}).start()
    for k in range(tokens // 128):
        v = own_ref[pl.ds(k * 128, 128), :].astype(F32)
        total = jnp.sum(v * v, axis=1, keepdims=True)
        ssg[me, :, pl.ds(k * 128, 128)] = jnp.broadcast_to(total, (128, 128)).T[0:8, :]
    for step in range(1, count):
        dev = lax.rem(me + step, count)
        remote(ssg.at[me], ssg.at[me], ssend.at[dev], srecv.at[me], {"tp": dev}).start()


def gather_finish(ring, xg, ssg, send, recv, ssend, srecv, count, pump):
    me = ring.me
    half = xg.shape[1] // 2
    a, b = pl.ds(0, half), pl.ds(half, half)
    right, left, far = ring.at(1), ring.at(-1), ring.at(2)

    def got(owner, rows, k):
        part = xg.at[owner, rows]
        remote(part, part, send.at[k], recv.at[k], {"tp": ring.sib}).wait_recv()
        return part

    def push(part, k, dev):
        remote(part, part, send.at[k], recv.at[k], {"tp": dev}).start()

    part = got(left, a, 0)
    push(part, 4, right)
    push(part, 7, ring.sib)
    part = got(right, b, 2)
    push(part, 5, left)
    push(part, 8, ring.sib)
    pump()
    push(got(left, b, 1), 9, ring.sib)
    push(got(right, a, 3), 10, ring.sib)
    pump()
    push(got(far, a, 4), 11, ring.sib)
    push(got(far, b, 5), 12, ring.sib)
    pump()
    whole = xg.at[ring.sib]
    remote(whole, whole, send.at[6], recv.at[6], {"tp": ring.sib}).wait()
    owners = {7: (-1, a), 8: (1, b), 9: (-1, b), 10: (1, a), 11: (2, a), 12: (2, b)}
    for k, (step, rows) in owners.items():
        part = xg.at[ring.at(step, other=True), rows]
        remote(part, part, send.at[k], recv.at[k], {"tp": ring.sib}).wait()
    for k in range(6):
        part = xg.at[me, a]
        remote(part, part, send.at[k], recv.at[k], {"tp": right}).wait_send()
    for step in range(1, count):
        dev = lax.rem(me + step, count)
        remote(ssg.at[dev], ssg.at[dev], ssend.at[dev], srecv.at[dev], {"tp": dev}).wait()


class Weights:
    def __init__(self, me, side, wvg, wo, gsend, grecv):
        self.y, self.z, self.side = lax.rem(me, side), me // side, side
        self.wvg, self.wo, self.gsend, self.grecv = wvg, wo, gsend, grecv
        self.waited = set()

    def idx(self, p, i, j):
        dy, dz = (i, j) if p == 0 else (j, i)
        return lax.rem(self.z + dz + self.side, self.side) * self.side + lax.rem(self.y + dy + self.side, self.side)

    def ref(self, unit, p, at):
        if unit % 2 == 0:
            return self.wvg.at[unit // 2, p, at]
        half = self.wo.shape[2] // 2
        return self.wo.at[unit // 2, at, pl.ds(p * half, half)]

    def push(self, unit, p, i, j, axis, d):
        ref = self.ref(unit, p, self.idx(p, i, j))
        di, dj = (d, 0) if axis == 0 else (0, d)
        slot = ((i - di) % 4) * 4 + (j - dj) % 4
        remote(
            ref, ref, self.gsend.at[2 * unit + p], self.grecv.at[2 * unit + p, slot], {"sp": self.idx(p, di, dj)}
        ).start()

    def arrive(self, unit, p, i, j):
        key = (unit, p, i % 4, j % 4)
        if key in self.waited or (i % 4, j % 4) == (0, 0):
            return
        self.waited.add(key)
        ref = self.ref(unit, p, self.idx(p, i, j))
        slot = (i % 4) * 4 + j % 4
        remote(
            ref, ref, self.gsend.at[2 * unit + p], self.grecv.at[2 * unit + p, slot], {"sp": self.idx(p, 1, 0)}
        ).wait_recv()

    def group(self, unit, p, i):
        for j in (0, -1, 1, 2):
            self.arrive(unit, p, i, j)

    def all(self, unit):
        for p in range(2):
            for i in (0, -1, 1, 2):
                self.group(unit, p, i)

    def opening(self, unit):
        for axis in range(2):
            for p in range(2):
                for d in (1, -1):
                    self.push(unit, p, 0, 0, axis, d)

    def events(self, unit):
        first = 1 if unit in (0, 3) else -1

        def turn(p, i, forward=None):
            def run():
                self.arrive(unit, p, i, 0)
                if forward:
                    self.push(unit, p, i, 0, 0, forward)
                for d in (1, -1):
                    self.push(unit, p, i, 0, 1, d)

            return run

        def relay(p, i):
            d = 1 if (i + unit) % 2 == 0 else -1

            def run():
                self.arrive(unit, p, i, -d)
                self.push(unit, p, i, -d, 1, d)

            return run

        both = range(2)
        early = [turn(p, -first, first) for p in both] + [turn(p, first) for p in both]
        early += [relay(p, 0) for p in both] + [turn(p, 2) for p in both]
        late = [relay(p, i) for i in (-1, 1) for p in both]
        last = [relay(p, 2) for p in both]
        return early, late, last

    def drain(self, unit):
        for p in range(2):
            if unit % 2 == 0:
                ref = self.wvg.at[unit // 2, p, pl.ds(0, 15)]
            else:
                half = self.wo.shape[2] // 2
                ref = self.wo.at[unit // 2, pl.ds(0, 15), pl.ds(p * half, half)]
            remote(ref, ref, self.gsend.at[2 * unit + p], self.grecv.at[2 * unit + p, 0], {"sp": self.idx(p, 1, 0)}).wait_send()


def whole_kernel(
    layers, n_sp, n_tp, features,
    stream_ref, gain_ref, wv_hbm, wg_hbm, wo_hbm, taps_ref, gates_ref, rate_ref, out,
    wvg, wo, xg, ssg, own, acc, mixb, mpad, sil, conv, convb, big, a_f, u_f, a_b, u_b, col,
    halo_p, halo_n, seg, ent, msg, slots,
    psend, precv, fbuf, far_in, nbuf, near_in,
    ld, gsend, grecv, asend, arecv, ssend, srecv, hsend, hrecv, csend, crecv, ds, dr, rs, rr,
):
    sp, tp = lax.axis_index("sp"), lax.axis_index("tp")
    tokens, width = mixb.shape
    feats = own.shape[1]
    ring = Ring(tp, n_tp)
    net = Weights(sp, 4, wvg, wo, gsend, grecv)
    pre = pown = big
    lanes_own = pl.ds(pl.multiple_of(tp * width, width), width)
    right, left = ring.at(1), ring.at(-1)

    loads = []
    for layer in range(layers):
        loads.append([
            pltpu.make_async_copy(wv_hbm.at[layer], wvg.at[layer, 0, sp], ld.at[3 * layer]),
            pltpu.make_async_copy(wg_hbm.at[layer], wvg.at[layer, 1, sp], ld.at[3 * layer + 1]),
        ])
        loads.append([pltpu.make_async_copy(wo_hbm.at[layer], wo.at[layer, sp], ld.at[3 * layer + 2])])
    for copies in loads:
        for copy in copies:
            copy.start()
    greet((("sp", n_sp, sp), ("tp", n_tp, tp)))

    queue = []

    def opening(unit):
        def run():
            for copy in loads[unit]:
                copy.wait()
            net.opening(unit)

        return run

    parts = [net.events(unit) for unit in range(2 * layers)]
    marks = {}
    queue.append(opening(0))
    for unit, (early, late, last) in enumerate(parts):
        queue.extend(early + late)
        if unit + 1 < len(parts):
            queue.append(opening(unit + 1))
        queue.extend(last)
        marks[unit] = len(queue)
    done = [0]

    def pump(n=1, upto=None):
        stop = min(done[0] + n, len(queue)) if upto is None else max(done[0], marks[upto])
        while done[0] < stop:
            queue[done[0]]()
            done[0] += 1

    def project(layer, p, i):
        def step(j, carry):
            at = net.idx(p, i, j)
            lanes = pl.ds(pl.multiple_of(lax.rem(at, 2) * 256, 256), 256)
            acc[p] += jnp.dot(xg[at // 2, :, lanes], wvg[layer, p, at], preferred_element_type=F32)
            return carry

        lax.fori_loop(0, 4, step, 0)

    def gather_begin(layer, source):
        gain = gain_ref[layer : layer + 1, lanes_own]
        gather_start(ring, source, gain, xg, ssg.at[layer], asend, arecv, ssend.at[layer], srecv.at[layer], n_tp)

    def gather_end(layer, count=1):
        gather_finish(
            ring, xg, ssg.at[layer], asend, arecv, ssend.at[layer], srecv.at[layer], n_tp, lambda: pump(count)
        )

    def column(layer):
        total = jnp.sum(ssg[layer], axis=0)
        scale = lax.rsqrt(total / features + NORM_EPS)
        for k in range(tokens // 128):
            part = jnp.broadcast_to(scale[0:1, k * 128 : (k + 1) * 128], (128, 128))
            col[pl.ds(k * 128, 128), :] = part.T

    def clear(rows):
        zero = jnp.zeros((rows.size, width), F32)
        acc[0, rows, :] = zero
        acc[1, rows, :] = zero

    def mix(layer):
        def finish_v(rows):
            wide = jnp.concatenate([col[rows, :]] * (width // 128), axis=1)
            value = (acc[0, rows, :] * wide).astype(BF16)
            mixb[rows, :] = value
            acc[0, rows, :] = value.astype(F32)

        in_row_steps(tokens, finish_v, 32)
        head, tail = mixb.at[pl.ds(0, 16)], mixb.at[pl.ds(tokens - 16, 16)]
        hs, hr = hsend.at[layer], hrecv.at[layer]
        to_next = remote(tail, halo_p.at[layer], hs.at[0], hr.at[0], {"sp": lax.rem(sp + 1, n_sp)})
        to_prev = remote(head, halo_n.at[layer], hs.at[1], hr.at[1], {"sp": lax.rem(sp + n_sp - 1, n_sp)})
        to_next.start()
        to_prev.start()

        def finish_g(rows):
            wide = jnp.concatenate([col[rows, :]] * (width // 128), axis=1)
            gate = (acc[1, rows, :] * wide).astype(BF16).astype(F32)
            sil[rows, :] = gate * sigmoid(gate)
            mpad[pl.ds(pl.multiple_of(rows.start + 16, 16), rows.size), :] = acc[0, rows, :]

        in_row_steps(tokens, finish_g, 32)
        pump(1)
        to_next.wait()
        to_prev.wait()
        sub = lax.broadcasted_iota(jnp.int32, (SEG, width), 0)
        before = halo_p[layer].astype(F32)
        after = halo_n[layer].astype(F32)
        for k in range(2):
            edge = jnp.where(sp > 0, before[8 * k + 7 : 8 * k + 8, :], 0.0)
            blk = acc[0, pl.ds(tokens - 16 + 8 * k, 8), :]
            mpad[pl.ds(8 * k, 8), :] = jnp.where(
                sub == 0, jnp.broadcast_to(edge, (SEG, width)), pltpu.roll(blk, 1, 0)
            )
        edge = jnp.where(sp < n_sp - 1, after[0:1, :], 0.0)
        blk = acc[0, pl.ds(0, 8), :]
        mpad[pl.ds(tokens + 16, 8), :] = jnp.where(
            sub == SEG - 1, jnp.broadcast_to(edge, (SEG, width)), pltpu.roll(blk, SEG - 1, 0)
        )
        taps = taps_ref[layer, :, lanes_own]

        def convolve(rows):
            terms = [
                mpad[pl.ds(pl.multiple_of(rows.start + 8 * k, 8), rows.size), :] * taps[k : k + 1, :]
                for k in range(4)
            ]
            value = (terms[0] + terms[1]) + (terms[2] + terms[3])
            conv[rows, :] = value
            convb[rows, :] = value.astype(BF16)

        in_row_steps(tokens, convolve, 32)
        for b in range(width // 128):
            maps = jnp.concatenate([gates_ref[layer, g, b] for g in range(4)], axis=1)
            pre[b] = jnp.dot(convb[:, b * 128 : (b + 1) * 128], maps, preferred_element_type=F32)
        pump(1)
        rate_all = -GATE_SCALE * rate_ref[layer, :, lanes_own]
        for b in range(width // 128):
            lanes = pl.ds(b * 128, 128)
            rates = [rate_all[e : e + 1, b * 128 : (b + 1) * 128] for e in range(2)]

            def body(k, carry, b=b, lanes=lanes, rates=rates):
                p_f, h_f, p_b, h_b = carry
                rows = pl.ds(pl.multiple_of(k * ROWS, ROWS), ROWS)
                cv = conv[rows, lanes]
                kept = []
                for e, (a_ref, u_ref) in enumerate(((a_f, u_f), (a_b, u_b))):
                    r = sigmoid(pre[b, rows, 256 * e : 256 * e + 128])
                    i = sigmoid(pre[b, rows, 256 * e + 128 : 256 * e + 256])
                    log_a = rates[e] * r
                    decay = jnp.exp(log_a)
                    drive = jnp.sqrt(drive_square(-2.0 * log_a)) * i * cv
                    a_ref[rows, lanes] = decay
                    u_ref[rows, lanes] = drive
                    kept.append((decay, drive))
                for j in range(ROWS // 8):
                    at = slice(8 * j, 8 * j + 8)
                    d, u = kept[0][0][at], kept[0][1][at]
                    h_f = d * h_f + u
                    p_f = p_f * d
                    d, u = kept[1][0][at], kept[1][1][at]
                    h_b = h_b + p_b * u
                    p_b = p_b * d
                return p_f, h_f, p_b, h_b

            one, zero = jnp.ones((SEG, 128), F32), jnp.zeros((SEG, 128), F32)
            ends = lax.fori_loop(0, tokens // ROWS, body, (one, zero, one, zero))
            for k in range(4):
                seg[k, :, lanes] = ends[k]
            pump(1)

        sides = ((0, range(SEG)), (2, range(SEG - 1, -1, -1)))
        for e, (k, order) in enumerate(sides):
            prod = jnp.ones((1, width), F32)
            state = jnp.zeros((1, width), F32)
            for s in order:
                d = seg[k, s : s + 1, :]
                state = d * state + seg[k + 1, s : s + 1, :]
                prod = prod * d
            for b in range(width // 128):
                msg[layer, e, b : b + 1, :] = prod[:, b * 128 : (b + 1) * 128]
                msg[layer, e, 4 + b : 5 + b, :] = state[:, b * 128 : (b + 1) * 128]
        cs, cr = csend.at[layer], crecv.at[layer]
        for step in range(1, n_sp):
            dev = lax.rem(sp + step, n_sp)
            side = jnp.where(dev > sp, 0, 1)
            remote(msg.at[layer, side], slots.at[layer, sp], cs.at[dev], cr.at[sp], {"sp": dev}).start()
        slots[layer, sp] = jnp.zeros((8, 128), F32)
        pump(1)
        for step in range(1, n_sp):
            dev = lax.rem(sp + step, n_sp)
            remote(msg.at[layer, 0], slots.at[layer, dev], cs.at[dev], cr.at[dev], {"sp": dev}).wait()
        for e, (k, order) in enumerate(sides):
            carry = jnp.zeros((4, 128), F32)
            for q in range(n_sp) if e == 0 else range(n_sp - 1, -1, -1):
                live = (q < sp) if e == 0 else (q > sp)
                slot = slots[layer, q]
                carry = jnp.where(live, slot[0:4] * carry + slot[4:8], carry)
            state = jnp.concatenate([carry[b : b + 1, :] for b in range(width // 128)], axis=1)
            for s in order:
                ent[e, s : s + 1, :] = state
                state = seg[k, s : s + 1, :] * state + seg[k + 1, s : s + 1, :]
        steps = tokens // SEG

        def again(k, carry):
            h_f, h_b = carry
            for j in range(4):
                fwd = pl.ds(pl.multiple_of((4 * k + j) * SEG, SEG), SEG)
                bwd = pl.ds(pl.multiple_of((steps - 1 - 4 * k - j) * SEG, SEG), SEG)
                h_f = a_f[fwd, :] * h_f + u_f[fwd, :]
                u_f[fwd, :] = h_f
                h_b = a_b[bwd, :] * h_b + u_b[bwd, :]
                u_b[bwd, :] = h_b
            return h_f, h_b

        lax.fori_loop(0, steps // 4, again, (ent[0], ent[1]))

        def gated(rows):
            mixb[rows, :] = ((u_f[rows, :] + u_b[rows, :]) * sil[rows, :]).astype(BF16)

        in_row_steps(tokens, gated, 32)

    half = tokens // 2
    top, low = pl.ds(0, half), pl.ds(half, half)

    def reduce(layer, source, target, count):
        order = (2, 1, -1, 0)

        def product(k, other):
            block = ring.at(order[k], other=other)
            terms = [
                lax.dot_general(
                    mixb[...], wo[layer, 2 * block + part], (((1,), (1,)), ((), ())), preferred_element_type=F32
                )
                for part in range(2)
            ]
            return terms

        def across(k):
            return remote(psend.at[k], precv.at[k], ds.at[k], dr.at[k], {"tp": ring.sib})

        def send(k, src, dst, dev):
            remote(src, dst, rs.at[k], rr.at[k], {"tp": dev}).start()

        def paired(k, rows, into=None):
            def body(r):
                at = pl.ds(pl.multiple_of(rows.start + r.start, 32), r.size)
                value = pown[k, at, :] + precv[k, at, :].astype(F32)
                if into is None:
                    pown[k, at, :] = value
                else:
                    into[at if into.shape[0] == tokens else r, :] = value.astype(BF16)

            in_row_steps(rows.size, body, 32)

        for k in range(4):
            for part, term in enumerate(product(k, True)):
                psend[k, :, part * 256 : (part + 1) * 256] = term.astype(BF16)
            across(k).start()
            for part, term in enumerate(product(k, False)):
                pown[k, :, part * 256 : (part + 1) * 256] = term
            if k == 1:
                across(0).wait_recv()
                paired(0, top, fbuf)
                send(0, fbuf.at[top], far_in.at[0], right)
                paired(0, low, fbuf)
                send(1, fbuf.at[low], far_in.at[1], left)
            if k == 2:
                across(1).wait_recv()
                paired(1, low, nbuf.at[0])
                send(2, nbuf.at[0], near_in.at[0], right)
                paired(1, top)
            if k == 3:
                across(2).wait_recv()
                paired(2, top, nbuf.at[1])
                send(3, nbuf.at[1], near_in.at[1], left)
                paired(2, low)
        across(3).wait_recv()
        paired(3, pl.ds(0, tokens))
        pump(count)

        def arrived(k, src, dst):
            remote(src, dst, rs.at[k], rr.at[k], {"tp": right}).wait_recv()

        def merged(k, rows, src, into):
            def body(r):
                at = pl.ds(pl.multiple_of(rows.start + r.start, 32), r.size)
                into[r, :] = (pown[k, at, :] + src[r, :].astype(F32)).astype(BF16)

            in_row_steps(half, body, 32)

        arrived(0, fbuf.at[top], far_in.at[0])
        merged(1, top, far_in.at[0], nbuf.at[2])
        send(4, nbuf.at[2], near_in.at[2], right)
        arrived(1, fbuf.at[low], far_in.at[1])
        merged(2, low, far_in.at[1], nbuf.at[3])
        send(5, nbuf.at[3], near_in.at[3], left)
        pump(count)
        for k in range(4):
            arrived(2 + k, nbuf.at[k], near_in.at[k])
            if k == 1:
                pump(count)

        def total(rows, one, two):
            def body(r):
                at = pl.ds(pl.multiple_of(rows.start + r.start, 32), r.size)
                branch = pown[3, at, :] + near_in[one, r, :].astype(F32) + near_in[two, r, :].astype(F32)
                target[at, :] = (source[at, :].astype(F32) + branch).astype(BF16)

            in_row_steps(half, body, 32)

        total(top, 1, 2)
        total(low, 0, 3)
        for k in range(4):
            across(k).wait_send()
        for k in range(6):
            remote(nbuf.at[0], near_in.at[0], rs.at[k], rr.at[k], {"tp": right}).wait_send()

    pump(1)
    gather_begin(0, stream_ref)
    in_row_steps(tokens, clear, 32)
    pump(2)
    gather_end(0, 2)
    column(0)
    for layer in range(layers):
        unit = 2 * layer
        if layer:
            pump(upto=unit)
        else:
            pump(len(parts[0][0]) + 1 - done[0])
        sets = [(i, p) for i in (0, -1, 1, 2) for p in range(2)]
        for n, (i, p) in enumerate(sets):
            if not layer:
                pump(1)
            net.group(unit, p, i)
            project(layer, p, i)
        mix(layer)
        pump(upto=unit + 1)
        net.all(unit + 1)
        if layer + 1 < layers:
            reduce(layer, stream_ref, own, 2)
            gather_begin(layer + 1, own)
            in_row_steps(tokens, clear, 32)
            gather_end(layer + 1, 2)
            column(layer + 1)
        else:
            reduce(layer, own, out, 0)
    for unit in range(2 * layers):
        net.drain(unit)


def whole_call(stream, gain, wv, wg, wo, taps, gates, rate, n_sp, n_tp):
    tokens, feats = stream.shape
    layers, rows, width = wv.shape
    half = tokens // 2
    blocks = width // 128
    vmem = pl.BlockSpec(memory_space=pltpu.VMEM)
    hbm = pl.BlockSpec(memory_space=pl.ANY)
    f32 = pltpu.VMEM((tokens, width), F32)
    b16 = pltpu.VMEM((tokens, width), BF16)
    dma = pltpu.SemaphoreType.DMA
    return pl.pallas_call(
        functools.partial(whole_kernel, layers, n_sp, n_tp, float(gain.shape[1])),
        out_shape=jax.ShapeDtypeStruct((tokens, feats), BF16),
        in_specs=[vmem, vmem, hbm, hbm, hbm, vmem, vmem, vmem],
        out_specs=vmem,
        scratch_shapes=[
            pltpu.VMEM((layers, 2, n_sp, rows, width), BF16),
            pltpu.VMEM((layers, n_sp, rows, width), BF16),
            pltpu.VMEM((n_tp, tokens, feats), BF16),
            pltpu.VMEM((layers, n_tp, 8, tokens), F32),
            b16,
            pltpu.VMEM((2, tokens, width), F32),
            b16,
            pltpu.VMEM((tokens + 24, width), F32),
            f32, f32, b16,
            pltpu.VMEM((4, tokens, 512), F32),
            f32, f32, f32, f32,
            pltpu.VMEM((tokens, 128), F32),
            pltpu.VMEM((layers, 16, width), BF16),
            pltpu.VMEM((layers, 16, width), BF16),
            pltpu.VMEM((4, SEG, width), F32),
            pltpu.VMEM((2, SEG, width), F32),
            pltpu.VMEM((layers, 2, 8, 128), F32),
            pltpu.VMEM((layers, n_sp, 8, 128), F32),
            pltpu.VMEM((4, tokens, feats), BF16),
            pltpu.VMEM((4, tokens, feats), BF16),
            pltpu.VMEM((tokens, feats), BF16),
            pltpu.VMEM((2, half, feats), BF16),
            pltpu.VMEM((4, half, feats), BF16),
            pltpu.VMEM((4, half, feats), BF16),
            dma((3 * layers,)),
            dma((4 * layers,)),
            dma((4 * layers, 16)),
            dma((13,)),
            dma((13,)),
            dma((layers, n_tp)),
            dma((layers, n_tp)),
            dma((layers, 2)),
            dma((layers, 2)),
            dma((layers, n_sp)),
            dma((layers, n_sp)),
            dma((4,)),
            dma((4,)),
            dma((6,)),
            dma((6,)),
        ],
        compiler_params=pltpu.CompilerParams(
            collective_id=0, has_side_effects=True, vmem_limit_bytes=63_000_000
        ),
        cost_estimate=pl.CostEstimate(flops=20_000_000_000, bytes_accessed=8_000_000, transcendentals=0),
        name="both_layers",
    )(stream, gain, wv, wg, wo, taps, gates, rate)


def per_device(
    n_sp, n_tp, stream_in, norm_gain, value_proj, gate_proj, out_proj, conv_taps, block_gates, forget_rate
):
    tokens, feats = stream_in.shape
    width = value_proj.shape[2]
    layers = value_proj.shape[0]
    steps = tokens // SEG
    gates = block_gates.reshape(layers, 4, width // 128, 128, 128)
    stream = stream_in.reshape(SEG, steps, feats).transpose(1, 0, 2).reshape(tokens, feats)
    stream = whole_call(
        stream, norm_gain, value_proj, gate_proj, out_proj, conv_taps, gates, forget_rate, n_sp, n_tp
    )
    return stream.reshape(steps, SEG, feats).transpose(1, 0, 2).reshape(tokens, feats)


def solution(mesh):
    placed = (
        P("sp", "tp"),
        P(),
        P(None, "sp", "tp"),
        P(None, "sp", "tp"),
        P(None, "sp", "tp"),
        P(),
        P(None, None, None, "tp", None),
        P(),
    )
    body = functools.partial(per_device, mesh.shape["sp"], mesh.shape["tp"])
    return jax.shard_map(body, mesh=mesh, in_specs=placed, out_specs=P("sp", "tp"), check_vma=False)
```

time: 761 us -> 217 us (0.29); the launches traced: 751 us -> 217 us
  waiting for transfers between devices: 238 us -> 0 us
  Pallas kernels: 0 us -> 212 us
  local copies, waits for them, and re-layouts: 215 us -> 4.12 us
  blocking collectives: 112 us -> 0 us
  other arithmetic: 83.9 us -> 0 us
  starting transfers between devices: 47.9 us -> 0 us
  matrix products: 36.7 us -> 0 us
  between operations: 17.1 us -> 0.01 us
    pallas_call x0 -> x1, Pallas kernels: none -> 212 us  [whole_call(): pl.pallas_call(functools.partial(whole_kernel, layers, n_sp, n_tp, float(...]
    all_gather x3 -> x0, waiting for transfers between devices: 212 us -> none  [the longest x1 156 us: in_one_piece(): out = lax.all_gather(both, axis, axis=dim, tiled=True)]
    slice x319 -> x0, local copies, waits for them, and re-layouts: 146 us -> none  [the longest x120 78 us: per_device(): lax.associative_scan(pair_combine, (fwd_decay, fwd_drive), axis=0)]
    all_to_all x2 -> x0, blocking collectives: 112 us -> none  [summed_on_arrival(): lax.all_to_all(blocks, axis, split_axis=0, concat_axis=0, tiled=True)]
    add x150 -> x0, other arithmetic: 40.6 us -> none  [the longest x72 22.9 us: pair_combine(): return (earlier[0] * latter[0], latter[0] * earlier[1] + latter[1])]
    all_to_all x6 -> x0, starting transfers between devices: 38.9 us -> none  [copy_for_each(): lax.all_to_all(jnp.broadcast_to(array[None], (count, *array.shape)), axis...]
    dot_general x8 -> x0, matrix products: 36.7 us -> none  [the longest x2 14.5 us: per_device(): proj_z = jnp.dot(piece, full_z, preferred_element_type=jnp.float32)]
    pad x128 -> x0, local copies, waits for them, and re-layouts: 33.5 us -> none  [the longest x64 27 us: per_device(): lax.associative_scan(pair_combine, (fwd_decay, fwd_drive), axis=0)]
  transfers between devices with their start and end apart: 13 -> 0, of which waited for: 11 -> 0; matrix products, arithmetic and copies ran while one was open for 3% -> 0% of each run, Pallas kernels for 0% -> 0%
where the time goes in v2:
time: 217 us
  Pallas kernels  212 us (98%)
  local copies, waits for them, and re-layouts  4.12 us (2%)
    pallas_call x1, Pallas kernels, whole_call(): pl.pallas_call(functools.partial(whole_kernel, layers, n_sp, n_tp, float(...  212 us

profile of v2, /device:TPU:1, one launch (start us, length us, event | category | flops | bytes accessed | tf_op | source)
XLA Modules:
  0.0 216.5 jit_solution(7119127923584235323)
XLA Ops:
  0.0 2.1 copy.12
  2.1 212.4 %both_layers.1 = bf16[512,512]{1,0:T(8,128)(2,1)} custom-call(bf16[512,512]{1,0:T(8,128)(2,1)} %bitcast.13, f32[2,4096]{1,0:T(2,128)} %gain_ref.1, bf16[2,256,512]{2,1,0:T(8,128)(2,1)} %wv_hbm.1, bf16[2,256,512]{2,1,0:T(8,128)(2,1)} %wg_hbm.1, bf16[2,256,512]{2,1,0:T(8,128)(2,1)} %wo_hbm.1, f32[2,4,4096]{2,1,0:T(4,128)} %taps_ref.1, ...), custom_call_target="tpu_custom_call" | custom-call | flops 20000000000 | bytes 8000000 | tf_op jit(solution)/shard_map/both_layers/pallas_call | solution.py:588
  214.5 2.0 copy.10

commit v3 on v2

--- a/solution.py
+++ b/solution.py
@@ -64,8 +64,7 @@
         return lax.rem(self.x + step + self.chips, self.chips) * 2 + core
 
 
-def gather_start(ring, own_ref, gain, xg, ssg, send, recv, ssend, srecv, count):
-    me = ring.me
+def gather_fill(own_ref, gain, xg, ssg, me):
     tokens = own_ref.shape[0]
 
     def fill(rows):
@@ -73,17 +72,21 @@
         xg[me, rows, :] = (v * gain).astype(BF16)
 
     in_row_steps(tokens, fill)
-    half = tokens // 2
+    for k in range(tokens // 128):
+        v = own_ref[pl.ds(k * 128, 128), :].astype(F32)
+        total = jnp.sum(v * v, axis=1, keepdims=True)
+        ssg[me, :, pl.ds(k * 128, 128)] = jnp.broadcast_to(total, (128, 128)).T[0:8, :]
+
+
+def gather_start(ring, xg, ssg, send, recv, ssend, srecv, count):
+    me = ring.me
+    half = xg.shape[1] // 2
     a, b = pl.ds(0, half), pl.ds(half, half)
     right, left = ring.at(1), ring.at(-1)
     for k, (rows, dev) in enumerate(((a, right), (b, right), (b, left), (a, left))):
         part = xg.at[me, rows]
         remote(part, part, send.at[k], recv.at[k], {"tp": dev}).start()
     remote(xg.at[me], xg.at[me], send.at[6], recv.at[6], {"tp": ring.sib}).start()
-    for k in range(tokens // 128):
-        v = own_ref[pl.ds(k * 128, 128), :].astype(F32)
-        total = jnp.sum(v * v, axis=1, keepdims=True)
-        ssg[me, :, pl.ds(k * 128, 128)] = jnp.broadcast_to(total, (128, 128)).T[0:8, :]
     for step in range(1, count):
         dev = lax.rem(me + step, count)
         remote(ssg.at[me], ssg.at[me], ssend.at[dev], srecv.at[me], {"tp": dev}).start()
@@ -203,11 +206,9 @@
             return run
 
         both = range(2)
-        early = [turn(p, -first, first) for p in both] + [turn(p, first) for p in both]
-        early += [relay(p, 0) for p in both] + [turn(p, 2) for p in both]
-        late = [relay(p, i) for i in (-1, 1) for p in both]
-        last = [relay(p, 2) for p in both]
-        return early, late, last
+        steps = [turn(p, -first, first) for p in both] + [turn(p, first) for p in both]
+        steps += [relay(p, 0) for p in both] + [turn(p, 2) for p in both]
+        return steps + [relay(p, i) for i in (-1, 1, 2) for p in both]
 
     def drain(self, unit):
         for p in range(2):
@@ -222,7 +223,7 @@
 def whole_kernel(
     layers, n_sp, n_tp, features,
     stream_ref, gain_ref, wv_hbm, wg_hbm, wo_hbm, taps_ref, gates_ref, rate_ref, out,
-    wvg, wo, xg, ssg, own, acc, mixb, mpad, sil, conv, convb, big, a_f, u_f, a_b, u_b, col,
+    wvg, wo, xg, ssg, base, own, perm, acc, mixb, mpad, sil, conv, convb, big, a_f, u_f, a_b, u_b, col,
     halo_p, halo_n, seg, ent, msg, slots,
     psend, precv, fbuf, far_in, nbuf, near_in,
     ld, gsend, grecv, asend, arecv, ssend, srecv, hsend, hrecv, csend, crecv, ds, dr, rs, rr,
@@ -246,8 +247,6 @@
     for copies in loads:
         for copy in copies:
             copy.start()
-    greet((("sp", n_sp, sp), ("tp", n_tp, tp)))
-
     queue = []
 
     def opening(unit):
@@ -258,19 +257,13 @@
 
         return run
 
-    parts = [net.events(unit) for unit in range(2 * layers)]
-    marks = {}
-    queue.append(opening(0))
-    for unit, (early, late, last) in enumerate(parts):
-        queue.extend(early + late)
-        if unit + 1 < len(parts):
-            queue.append(opening(unit + 1))
-        queue.extend(last)
-        marks[unit] = len(queue)
+    for unit in range(2 * layers):
+        queue.append(opening(unit))
+        queue.extend(net.events(unit))
     done = [0]
 
-    def pump(n=1, upto=None):
-        stop = min(done[0] + n, len(queue)) if upto is None else max(done[0], marks[upto])
+    def pump(n):
+        stop = min(done[0] + n, len(queue))
         while done[0] < stop:
             queue[done[0]]()
             done[0] += 1
@@ -282,15 +275,37 @@
             acc[p] += jnp.dot(xg[at // 2, :, lanes], wvg[layer, p, at], preferred_element_type=F32)
             return carry
 
-        lax.fori_loop(0, 4, step, 0)
-
-    def gather_begin(layer, source):
+        def pair(j, carry):
+            block = lax.rem(net.z + i + net.side, net.side) * 2 + j
+            both = wvg[layer, p, pl.ds(2 * block, 2)].reshape(feats, width)
+            acc[p] += jnp.dot(xg[block], both, preferred_element_type=F32)
+            return carry
+
+        if p == 0:
+            lax.fori_loop(0, 4, step, 0)
+        else:
+            lax.fori_loop(0, 2, pair, 0)
+
+    def project_all(layer):
+        def step(block, carry):
+            for p in range(2):
+                both = wvg[layer, p, pl.ds(2 * block, 2)].reshape(feats, width)
+                acc[p] += jnp.dot(xg[block], both, preferred_element_type=F32)
+            return carry
+
+        lax.fori_loop(0, n_tp, step, 0)
+
+    def gather_own(layer, source):
         gain = gain_ref[layer : layer + 1, lanes_own]
-        gather_start(ring, source, gain, xg, ssg.at[layer], asend, arecv, ssend.at[layer], srecv.at[layer], n_tp)
-
-    def gather_end(layer, count=1):
+        gather_fill(source, gain, xg, ssg.at[layer], tp)
+
+    def gather_begin(layer):
+        gather_start(ring, xg, ssg.at[layer], asend, arecv, ssend.at[layer], srecv.at[layer], n_tp)
+
+    def gather_end(layer, counts):
+        pumps = iter(counts)
         gather_finish(
-            ring, xg, ssg.at[layer], asend, arecv, ssend.at[layer], srecv.at[layer], n_tp, lambda: pump(count)
+            ring, xg, ssg.at[layer], asend, arecv, ssend.at[layer], srecv.at[layer], n_tp, lambda: pump(next(pumps))
         )
 
     def column(layer):
@@ -327,7 +342,7 @@
             mpad[pl.ds(pl.multiple_of(rows.start + 16, 16), rows.size), :] = acc[0, rows, :]
 
         in_row_steps(tokens, finish_g, 32)
-        pump(1)
+        pump(2)
         to_next.wait()
         to_prev.wait()
         sub = lax.broadcasted_iota(jnp.int32, (SEG, width), 0)
@@ -359,7 +374,7 @@
         for b in range(width // 128):
             maps = jnp.concatenate([gates_ref[layer, g, b] for g in range(4)], axis=1)
             pre[b] = jnp.dot(convb[:, b * 128 : (b + 1) * 128], maps, preferred_element_type=F32)
-        pump(1)
+        pump(2)
         rate_all = -GATE_SCALE * rate_ref[layer, :, lanes_own]
         for b in range(width // 128):
             lanes = pl.ds(b * 128, 128)
@@ -393,7 +408,8 @@
             ends = lax.fori_loop(0, tokens // ROWS, body, (one, zero, one, zero))
             for k in range(4):
                 seg[k, :, lanes] = ends[k]
-            pump(1)
+            if b in (0, 3):
+                pump(2)
 
         sides = ((0, range(SEG)), (2, range(SEG - 1, -1, -1)))
         for e, (k, order) in enumerate(sides):
@@ -412,7 +428,7 @@
             side = jnp.where(dev > sp, 0, 1)
             remote(msg.at[layer, side], slots.at[layer, sp], cs.at[dev], cr.at[sp], {"sp": dev}).start()
         slots[layer, sp] = jnp.zeros((8, 128), F32)
-        pump(1)
+        pump(4)
         for step in range(1, n_sp):
             dev = lax.rem(sp + step, n_sp)
             remote(msg.at[layer, 0], slots.at[layer, dev], cs.at[dev], cr.at[dev], {"sp": dev}).wait()
@@ -426,8 +442,6 @@
             for s in order:
                 ent[e, s : s + 1, :] = state
                 state = seg[k, s : s + 1, :] * state + seg[k + 1, s : s + 1, :]
-        steps = tokens // SEG
-
         def again(k, carry):
             h_f, h_b = carry
             for j in range(4):
@@ -449,7 +463,7 @@
     half = tokens // 2
     top, low = pl.ds(0, half), pl.ds(half, half)
 
-    def reduce(layer, source, target, count):
+    def reduce(layer, source, target, counts):
         order = (2, 1, -1, 0)
 
         def product(k, other):
@@ -503,7 +517,7 @@
                 paired(2, low)
         across(3).wait_recv()
         paired(3, pl.ds(0, tokens))
-        pump(count)
+        pump(counts[0])
 
         def arrived(k, src, dst):
             remote(src, dst, rs.at[k], rr.at[k], {"tp": right}).wait_recv()
@@ -521,17 +535,25 @@
         arrived(1, fbuf.at[low], far_in.at[1])
         merged(2, low, far_in.at[1], nbuf.at[3])
         send(5, nbuf.at[3], near_in.at[3], left)
-        pump(count)
+        pump(counts[1])
         for k in range(4):
             arrived(2 + k, nbuf.at[k], near_in.at[k])
             if k == 1:
-                pump(count)
+                pump(counts[2])
 
         def total(rows, one, two):
             def body(r):
                 at = pl.ds(pl.multiple_of(rows.start + r.start, 32), r.size)
                 branch = pown[3, at, :] + near_in[one, r, :].astype(F32) + near_in[two, r, :].astype(F32)
-                target[at, :] = (source[at, :].astype(F32) + branch).astype(BF16)
+                value = source[at, :].astype(F32) + branch
+                if target is None:
+                    for j in range(r.size // SEG):
+                        for b in range(feats // 128):
+                            perm[b, pl.ds(at.start // SEG + j, SEG, stride=steps), :] = value[
+                                j * SEG : (j + 1) * SEG, b * 128 : (b + 1) * 128
+                            ]
+                else:
+                    target[at, :] = value.astype(BF16)
 
             in_row_steps(half, body, 32)
 
@@ -542,35 +564,59 @@
         for k in range(6):
             remote(nbuf.at[0], near_in.at[0], rs.at[k], rr.at[k], {"tp": right}).wait_send()
 
+    steps = tokens // SEG
+
+    def spread(rows):
+        for b in range(feats // 128):
+            perm[b, rows, :] = stream_ref[rows, b * 128 : (b + 1) * 128].astype(F32)
+
+    def collect(rows):
+        first = rows.start // SEG
+        for b in range(feats // 128):
+            parts = [perm[b, pl.ds(first + j, SEG, stride=steps), :] for j in range(rows.size // SEG)]
+            base[rows, b * 128 : (b + 1) * 128] = jnp.concatenate(parts, axis=0).astype(BF16)
+
+    def finish(rows):
+        for b in range(feats // 128):
+            out[rows, b * 128 : (b + 1) * 128] = perm[b, rows, :].astype(BF16)
+
+    in_row_steps(tokens, spread)
+    in_row_steps(tokens, collect, 32)
+    gather_own(0, base)
+    greet((("sp", n_sp, sp), ("tp", n_tp, tp)))
+
     pump(1)
-    gather_begin(0, stream_ref)
+    gather_begin(0)
     in_row_steps(tokens, clear, 32)
-    pump(2)
-    gather_end(0, 2)
+    gather_end(0, (4, 2, 2))
     column(0)
     for layer in range(layers):
         unit = 2 * layer
         if layer:
-            pump(upto=unit)
+            net.all(unit)
+            project_all(layer)
         else:
-            pump(len(parts[0][0]) + 1 - done[0])
-        sets = [(i, p) for i in (0, -1, 1, 2) for p in range(2)]
-        for n, (i, p) in enumerate(sets):
-            if not layer:
-                pump(1)
-            net.group(unit, p, i)
-            project(layer, p, i)
+            pump(4)
+            for i in (0, -1, 1, 2):
+                for p in range(2):
+                    net.group(unit, p, i)
+                    project(layer, p, i)
+                if i == 0:
+                    pump(3)
         mix(layer)
-        pump(upto=unit + 1)
+        pump(3)
         net.all(unit + 1)
         if layer + 1 < layers:
-            reduce(layer, stream_ref, own, 2)
-            gather_begin(layer + 1, own)
+            reduce(layer, base, own, (0, 4, 2))
+            gather_own(layer + 1, own)
+            gather_begin(layer + 1)
+            pump(2)
             in_row_steps(tokens, clear, 32)
-            gather_end(layer + 1, 2)
+            gather_end(layer + 1, (2, 2, 3))
             column(layer + 1)
         else:
-            reduce(layer, own, out, 0)
+            reduce(layer, own, None, (0, 0, 0))
+            in_row_steps(tokens, finish)
     for unit in range(2 * layers):
         net.drain(unit)
 
@@ -595,7 +641,8 @@
             pltpu.VMEM((layers, n_sp, rows, width), BF16),
             pltpu.VMEM((n_tp, tokens, feats), BF16),
             pltpu.VMEM((layers, n_tp, 8, tokens), F32),
-            b16,
+            b16, b16,
+            pltpu.VMEM((feats // 128, tokens, 128), F32),
             pltpu.VMEM((2, tokens, width), F32),
             b16,
             pltpu.VMEM((tokens + 24, width), F32),
@@ -642,16 +689,12 @@
 def per_device(
     n_sp, n_tp, stream_in, norm_gain, value_proj, gate_proj, out_proj, conv_taps, block_gates, forget_rate
 ):
-    tokens, feats = stream_in.shape
     width = value_proj.shape[2]
     layers = value_proj.shape[0]
-    steps = tokens // SEG
     gates = block_gates.reshape(layers, 4, width // 128, 128, 128)
-    stream = stream_in.reshape(SEG, steps, feats).transpose(1, 0, 2).reshape(tokens, feats)
-    stream = whole_call(
-        stream, norm_gain, value_proj, gate_proj, out_proj, conv_taps, gates, forget_rate, n_sp, n_tp
+    return whole_call(
+        stream_in, norm_gain, value_proj, gate_proj, out_proj, conv_taps, gates, forget_rate, n_sp, n_tp
     )
-    return stream.reshape(steps, SEG, feats).transpose(1, 0, 2).reshape(tokens, feats)
 
 
 def solution(mesh):

time: 217 us -> 193 us (0.89)
  Pallas kernels: 212 us -> 191 us
  local copies, waits for them, and re-layouts: 4.12 us -> 1.87 us
    pallas_call x1, Pallas kernels: 212 us -> 191 us  [whole_call(): pl.pallas_call(functools.partial(whole_kernel, layers, n_sp, n_tp, float(...]
where the time goes in v3:
time: 193 us
  Pallas kernels  191 us (99%)
    pallas_call x1, Pallas kernels, whole_call(): pl.pallas_call(functools.partial(whole_kernel, layers, n_sp, n_tp, float(...  191 us

profile of v3, /device:TPU:1, one launch (start us, length us, event | category | flops | bytes accessed | tf_op | source)
XLA Modules:
  0.0 193.2 jit_solution(14848592530264155784)
XLA Ops:
  0.0 191.3 %both_layers.1 = bf16[512,512]{1,0:T(8,128)(2,1)} custom-call(bf16[512,512]{1,0:T(8,128)(2,1)} %stream_ref.1, f32[2,4096]{1,0:T(2,128)} %gain_ref.1, bf16[2,256,512]{2,1,0:T(8,128)(2,1)} %wv_hbm.1, bf16[2,256,512]{2,1,0:T(8,128)(2,1)} %wg_hbm.1, bf16[2,256,512]{2,1,0:T(8,128)(2,1)} %wo_hbm.1, f32[2,4,4096]{2,1,0:T(4,128)} %taps_ref.1, ...), custom_call_target="tpu_custom_call" | custom-call | flops 20000000000 | bytes 8000000 | tf_op jit(solution)/shard_map/both_layers/pallas_call | solution.py:634
  191.3 1.9 copy.10

commit v4 on v3

--- a/solution.py
+++ b/solution.py
@@ -14,6 +14,7 @@
 BF16 = jnp.bfloat16
 SEG = 8
 ROWS = 64
+PLAN = ('000', '00', '0', '000', '01', '000', '', '', '', '01', '01', '', '11111', '', '11111', '', '', '', '1', '', '1', '2', '', '3', '2', '', '2', '2', '2', '', '2', '2', '2', '2', '2', '2', '223', '2', '', '', '2', '3', '', '333', '', '', '', '', '33', '3', '3', '', '33', '', '3', '33', '', '', '', '', '', '', '', '')
 
 
 def remote(src, dst, send_sem, recv_sem, dev):
@@ -27,7 +28,7 @@
     for axis, count, me in groups:
         for step in range(1, count):
             pl.semaphore_signal(barrier, inc=1, device_id={axis: lax.rem(me + step, count)}, device_id_type=MESH)
-    pl.semaphore_wait(barrier, sum(count - 1 for _, count, _ in groups))
+    return lambda: pl.semaphore_wait(barrier, sum(count - 1 for _, count, _ in groups))
 
 
 def sigmoid(v):
@@ -42,12 +43,16 @@
     return total * y
 
 
-def in_row_steps(rows, body, size=ROWS):
+def in_row_steps(rows, body, size=ROWS, first=0):
     def step(k, carry):
-        body(pl.ds(pl.multiple_of(k * size, size), size))
+        body(pl.ds(pl.multiple_of(first + k * size, size), size))
         return carry
 
     lax.fori_loop(0, rows // size, step, 0)
+
+
+def aligned(at, size):
+    return at if isinstance(at, int) else pl.multiple_of(at, size)
 
 
 class Ring:
@@ -64,73 +69,74 @@
         return lax.rem(self.x + step + self.chips, self.chips) * 2 + core
 
 
-def gather_fill(own_ref, gain, xg, ssg, me):
+def gather_fill(own_ref, gain, xg, ssg, me, half=None):
     tokens = own_ref.shape[0]
+    first, count = (0, tokens) if half is None else (half * tokens // 2, tokens // 2)
 
     def fill(rows):
-        v = own_ref[rows, :].astype(F32)
-        xg[me, rows, :] = (v * gain).astype(BF16)
-
-    in_row_steps(tokens, fill)
-    for k in range(tokens // 128):
+        at = pl.ds(pl.multiple_of(first + rows.start, ROWS), rows.size)
+        v = own_ref[at, :].astype(F32)
+        xg[me, at, :] = (v * gain).astype(BF16)
+
+    in_row_steps(count, fill)
+    for k in range(first // 128, (first + count) // 128):
         v = own_ref[pl.ds(k * 128, 128), :].astype(F32)
         total = jnp.sum(v * v, axis=1, keepdims=True)
         ssg[me, :, pl.ds(k * 128, 128)] = jnp.broadcast_to(total, (128, 128)).T[0:8, :]
 
 
-def gather_start(ring, xg, ssg, send, recv, ssend, srecv, count):
-    me = ring.me
-    half = xg.shape[1] // 2
-    a, b = pl.ds(0, half), pl.ds(half, half)
-    right, left = ring.at(1), ring.at(-1)
-    for k, (rows, dev) in enumerate(((a, right), (b, right), (b, left), (a, left))):
-        part = xg.at[me, rows]
-        remote(part, part, send.at[k], recv.at[k], {"tp": dev}).start()
-    remote(xg.at[me], xg.at[me], send.at[6], recv.at[6], {"tp": ring.sib}).start()
-    for step in range(1, count):
-        dev = lax.rem(me + step, count)
-        remote(ssg.at[me], ssg.at[me], ssend.at[dev], srecv.at[me], {"tp": dev}).start()
-
-
-def gather_finish(ring, xg, ssg, send, recv, ssend, srecv, count, pump):
-    me = ring.me
-    half = xg.shape[1] // 2
-    a, b = pl.ds(0, half), pl.ds(half, half)
-    right, left, far = ring.at(1), ring.at(-1), ring.at(2)
-
-    def got(owner, rows, k):
-        part = xg.at[owner, rows]
-        remote(part, part, send.at[k], recv.at[k], {"tp": ring.sib}).wait_recv()
-        return part
-
-    def push(part, k, dev):
-        remote(part, part, send.at[k], recv.at[k], {"tp": dev}).start()
-
-    part = got(left, a, 0)
-    push(part, 4, right)
-    push(part, 7, ring.sib)
-    part = got(right, b, 2)
-    push(part, 5, left)
-    push(part, 8, ring.sib)
-    pump()
-    push(got(left, b, 1), 9, ring.sib)
-    push(got(right, a, 3), 10, ring.sib)
-    pump()
-    push(got(far, a, 4), 11, ring.sib)
-    push(got(far, b, 5), 12, ring.sib)
-    pump()
-    whole = xg.at[ring.sib]
-    remote(whole, whole, send.at[6], recv.at[6], {"tp": ring.sib}).wait()
-    owners = {7: (-1, a), 8: (1, b), 9: (-1, b), 10: (1, a), 11: (2, a), 12: (2, b)}
-    for k, (step, rows) in owners.items():
-        part = xg.at[ring.at(step, other=True), rows]
-        remote(part, part, send.at[k], recv.at[k], {"tp": ring.sib}).wait()
-    for k in range(6):
-        part = xg.at[me, a]
-        remote(part, part, send.at[k], recv.at[k], {"tp": right}).wait_send()
-    for step in range(1, count):
-        dev = lax.rem(me + step, count)
-        remote(ssg.at[dev], ssg.at[dev], ssend.at[dev], srecv.at[dev], {"tp": dev}).wait()
+class Gather:
+    def __init__(self, ring, xg, ssg, send, recv, ssend, srecv, count):
+        self.ring, self.xg, self.ssg, self.count = ring, xg, ssg, count
+        self.send, self.recv, self.ssend, self.srecv = send, recv, ssend, srecv
+        half = xg.shape[1] // 2
+        self.rows = (pl.ds(0, half), pl.ds(half, half))
+
+    def push(self, part, k, dev):
+        remote(part, part, self.send.at[k], self.recv.at[k], {"tp": dev}).start()
+
+    def begin(self, half):
+        ring = self.ring
+        part = self.xg.at[ring.me, self.rows[half]]
+        right, left = ring.at(1), ring.at(-1)
+        if half == 0:
+            self.push(part, 0, right)
+            self.push(part, 3, left)
+            self.push(part, 6, ring.sib)
+        else:
+            self.push(part, 2, left)
+            self.push(part, 1, right)
+            self.push(part, 13, ring.sib)
+
+    def begin_squares(self):
+        ring, ssg = self.ring, self.ssg
+        for step in range(1, self.count):
+            dev = lax.rem(ring.me + step, self.count)
+            remote(ssg.at[ring.me], ssg.at[ring.me], self.ssend.at[dev], self.srecv.at[ring.me], {"tp": dev}).start()
+
+    def got(self, k):
+        ring = self.ring
+        step, half = {0: (-1, 0), 1: (-1, 1), 2: (1, 1), 3: (1, 0), 4: (2, 0), 5: (2, 1)}[k]
+        part = self.xg.at[ring.at(step), self.rows[half]]
+        remote(part, part, self.send.at[k], self.recv.at[k], {"tp": ring.sib}).wait_recv()
+        if k == 0:
+            self.push(part, 4, ring.at(1))
+        if k == 2:
+            self.push(part, 5, ring.at(-1))
+        self.push(part, 7 + k, ring.sib)
+
+    def end(self):
+        ring = self.ring
+        owners = {6: (0, 0), 13: (0, 1), 7: (-1, 0), 8: (-1, 1), 9: (1, 1), 10: (1, 0), 11: (2, 0), 12: (2, 1)}
+        for k, (step, half) in owners.items():
+            part = self.xg.at[ring.at(step, other=True), self.rows[half]]
+            remote(part, part, self.send.at[k], self.recv.at[k], {"tp": ring.sib}).wait()
+        for k in range(6):
+            part = self.xg.at[ring.me, self.rows[0]]
+            remote(part, part, self.send.at[k], self.recv.at[k], {"tp": ring.at(1)}).wait_send()
+        for step in range(1, self.count):
+            dev = lax.rem(ring.me + step, self.count)
+            remote(self.ssg.at[dev], self.ssg.at[dev], self.ssend.at[dev], self.srecv.at[dev], {"tp": dev}).wait()
 
 
 class Weights:
@@ -231,6 +237,7 @@
     sp, tp = lax.axis_index("sp"), lax.axis_index("tp")
     tokens, width = mixb.shape
     feats = own.shape[1]
+    joined = greet((("sp", n_sp, sp), ("tp", n_tp, tp)))
     ring = Ring(tp, n_tp)
     net = Weights(sp, 4, wvg, wo, gsend, grecv)
     pre = pown = big
@@ -247,66 +254,46 @@
     for copies in loads:
         for copy in copies:
             copy.start()
-    queue = []
-
     def opening(unit):
-        def run():
-            for copy in loads[unit]:
-                copy.wait()
-            net.opening(unit)
-
-        return run
-
-    for unit in range(2 * layers):
-        queue.append(opening(unit))
-        queue.extend(net.events(unit))
-    done = [0]
-
-    def pump(n):
-        stop = min(done[0] + n, len(queue))
-        while done[0] < stop:
-            queue[done[0]]()
-            done[0] += 1
+        for copy in loads[unit]:
+            copy.wait()
+        net.opening(unit)
+
+    waiting = [iter([functools.partial(opening, unit)] + net.events(unit)) for unit in range(2 * layers)]
+    plan = iter(PLAN)
+
+    def slot():
+        for unit in next(plan):
+            next(waiting[int(unit)])()
 
     def project(layer, p, i):
-        def step(j, carry):
-            at = net.idx(p, i, j)
-            lanes = pl.ds(pl.multiple_of(lax.rem(at, 2) * 256, 256), 256)
-            acc[p] += jnp.dot(xg[at // 2, :, lanes], wvg[layer, p, at], preferred_element_type=F32)
-            return carry
-
-        def pair(j, carry):
-            block = lax.rem(net.z + i + net.side, net.side) * 2 + j
-            both = wvg[layer, p, pl.ds(2 * block, 2)].reshape(feats, width)
-            acc[p] += jnp.dot(xg[block], both, preferred_element_type=F32)
-            return carry
-
         if p == 0:
-            lax.fori_loop(0, 4, step, 0)
+            spots = [net.idx(p, i, j) for j in range(4)]
+            halves = [pl.ds(pl.multiple_of(lax.rem(at, 2) * 256, 256), 256) for at in spots]
+            terms = [
+                jnp.dot(xg[at // 2, :, lanes], wvg[layer, p, at], preferred_element_type=F32)
+                for at, lanes in zip(spots, halves)
+            ]
         else:
-            lax.fori_loop(0, 2, pair, 0)
-
-    def project_all(layer):
-        def step(block, carry):
-            for p in range(2):
-                both = wvg[layer, p, pl.ds(2 * block, 2)].reshape(feats, width)
-                acc[p] += jnp.dot(xg[block], both, preferred_element_type=F32)
-            return carry
-
-        lax.fori_loop(0, n_tp, step, 0)
-
-    def gather_own(layer, source):
+            first = lax.rem(net.z + i + net.side, net.side) * 2
+            terms = [
+                jnp.dot(
+                    xg[first + j],
+                    wvg[layer, p, pl.ds(2 * (first + j), 2)].reshape(feats, width),
+                    preferred_element_type=F32,
+                )
+                for j in range(2)
+            ]
+        acc[p] += functools.reduce(jnp.add, terms)
+
+    gathers = [
+        Gather(ring, xg, ssg.at[layer], asend, arecv, ssend.at[layer], srecv.at[layer], n_tp)
+        for layer in range(layers)
+    ]
+
+    def gather_own(layer, source, half=None):
         gain = gain_ref[layer : layer + 1, lanes_own]
-        gather_fill(source, gain, xg, ssg.at[layer], tp)
-
-    def gather_begin(layer):
-        gather_start(ring, xg, ssg.at[layer], asend, arecv, ssend.at[layer], srecv.at[layer], n_tp)
-
-    def gather_end(layer, counts):
-        pumps = iter(counts)
-        gather_finish(
-            ring, xg, ssg.at[layer], asend, arecv, ssend.at[layer], srecv.at[layer], n_tp, lambda: pump(next(pumps))
-        )
+        gather_fill(source, gain, xg, ssg.at[layer], tp, half)
 
     def column(layer):
         total = jnp.sum(ssg[layer], axis=0)
@@ -327,7 +314,8 @@
             mixb[rows, :] = value
             acc[0, rows, :] = value.astype(F32)
 
-        in_row_steps(tokens, finish_v, 32)
+        finish_v(pl.ds(0, 32))
+        finish_v(pl.ds(tokens - 32, 32))
         head, tail = mixb.at[pl.ds(0, 16)], mixb.at[pl.ds(tokens - 16, 16)]
         hs, hr = hsend.at[layer], hrecv.at[layer]
         to_next = remote(tail, halo_p.at[layer], hs.at[0], hr.at[0], {"sp": lax.rem(sp + 1, n_sp)})
@@ -339,10 +327,30 @@
             wide = jnp.concatenate([col[rows, :]] * (width // 128), axis=1)
             gate = (acc[1, rows, :] * wide).astype(BF16).astype(F32)
             sil[rows, :] = gate * sigmoid(gate)
-            mpad[pl.ds(pl.multiple_of(rows.start + 16, 16), rows.size), :] = acc[0, rows, :]
-
+            mpad[pl.ds(aligned(rows.start + 16, 16), rows.size), :] = acc[0, rows, :]
+
+        in_row_steps(tokens - 64, finish_v, 32, 32)
         in_row_steps(tokens, finish_g, 32)
-        pump(2)
+        taps = taps_ref[layer, :, lanes_own]
+        maps = [jnp.concatenate([gates_ref[layer, g, b] for g in range(4)], axis=1) for b in range(width // 128)]
+        quarter = tokens // 4
+
+        def gate_maps(rows):
+            for b in range(width // 128):
+                pre[b, rows, :] = jnp.dot(convb[rows, b * 128 : (b + 1) * 128], maps[b], preferred_element_type=F32)
+
+        def convolve(rows):
+            terms = [
+                mpad[pl.ds(aligned(rows.start + 8 * k, 8), rows.size), :] * taps[k : k + 1, :]
+                for k in range(4)
+            ]
+            value = (terms[0] + terms[1]) + (terms[2] + terms[3])
+            conv[rows, :] = value
+            convb[rows, :] = value.astype(BF16)
+
+        in_row_steps(tokens - 64, convolve, 32, 32)
+        gate_maps(pl.ds(quarter, 2 * quarter))
+        slot()
         to_next.wait()
         to_prev.wait()
         sub = lax.broadcasted_iota(jnp.int32, (SEG, width), 0)
@@ -359,22 +367,12 @@
         mpad[pl.ds(tokens + 16, 8), :] = jnp.where(
             sub == SEG - 1, jnp.broadcast_to(edge, (SEG, width)), pltpu.roll(blk, SEG - 1, 0)
         )
-        taps = taps_ref[layer, :, lanes_own]
-
-        def convolve(rows):
-            terms = [
-                mpad[pl.ds(pl.multiple_of(rows.start + 8 * k, 8), rows.size), :] * taps[k : k + 1, :]
-                for k in range(4)
-            ]
-            value = (terms[0] + terms[1]) + (terms[2] + terms[3])
-            conv[rows, :] = value
-            convb[rows, :] = value.astype(BF16)
-
-        in_row_steps(tokens, convolve, 32)
-        for b in range(width // 128):
-            maps = jnp.concatenate([gates_ref[layer, g, b] for g in range(4)], axis=1)
-            pre[b] = jnp.dot(convb[:, b * 128 : (b + 1) * 128], maps, preferred_element_type=F32)
-        pump(2)
+        convolve(pl.ds(0, 32))
+        convolve(pl.ds(tokens - 32, 32))
+        slot()
+        gate_maps(pl.ds(0, quarter))
+        gate_maps(pl.ds(3 * quarter, quarter))
+        slot()
         rate_all = -GATE_SCALE * rate_ref[layer, :, lanes_own]
         for b in range(width // 128):
             lanes = pl.ds(b * 128, 128)
@@ -408,8 +406,7 @@
             ends = lax.fori_loop(0, tokens // ROWS, body, (one, zero, one, zero))
             for k in range(4):
                 seg[k, :, lanes] = ends[k]
-            if b in (0, 3):
-                pump(2)
+            slot()
 
         sides = ((0, range(SEG)), (2, range(SEG - 1, -1, -1)))
         for e, (k, order) in enumerate(sides):
@@ -428,7 +425,7 @@
             side = jnp.where(dev > sp, 0, 1)
             remote(msg.at[layer, side], slots.at[layer, sp], cs.at[dev], cr.at[sp], {"sp": dev}).start()
         slots[layer, sp] = jnp.zeros((8, 128), F32)
-        pump(4)
+        slot()
         for step in range(1, n_sp):
             dev = lax.rem(sp + step, n_sp)
             remote(msg.at[layer, 0], slots.at[layer, dev], cs.at[dev], cr.at[dev], {"sp": dev}).wait()
@@ -436,8 +433,8 @@
             carry = jnp.zeros((4, 128), F32)
             for q in range(n_sp) if e == 0 else range(n_sp - 1, -1, -1):
                 live = (q < sp) if e == 0 else (q > sp)
-                slot = slots[layer, q]
-                carry = jnp.where(live, slot[0:4] * carry + slot[4:8], carry)
+                entry = slots[layer, q]
+                carry = jnp.where(live, entry[0:4] * carry + entry[4:8], carry)
             state = jnp.concatenate([carry[b : b + 1, :] for b in range(width // 128)], axis=1)
             for s in order:
                 ent[e, s : s + 1, :] = state
@@ -459,11 +456,12 @@
             mixb[rows, :] = ((u_f[rows, :] + u_b[rows, :]) * sil[rows, :]).astype(BF16)
 
         in_row_steps(tokens, gated, 32)
+        slot()
 
     half = tokens // 2
     top, low = pl.ds(0, half), pl.ds(half, half)
 
-    def reduce(layer, source, target, counts):
+    def reduce(layer, source, target, chained):
         order = (2, 1, -1, 0)
 
         def product(k, other):
@@ -508,16 +506,18 @@
             if k == 2:
                 across(1).wait_recv()
                 paired(1, low, nbuf.at[0])
-                send(2, nbuf.at[0], near_in.at[0], right)
+                if not chained:
+                    send(2, nbuf.at[0], near_in.at[0], right)
                 paired(1, top)
             if k == 3:
                 across(2).wait_recv()
                 paired(2, top, nbuf.at[1])
                 send(3, nbuf.at[1], near_in.at[1], left)
                 paired(2, low)
+            slot()
         across(3).wait_recv()
         paired(3, pl.ds(0, tokens))
-        pump(counts[0])
+        slot()
 
         def arrived(k, src, dst):
             remote(src, dst, rs.at[k], rr.at[k], {"tp": right}).wait_recv()
@@ -532,33 +532,49 @@
         arrived(0, fbuf.at[top], far_in.at[0])
         merged(1, top, far_in.at[0], nbuf.at[2])
         send(4, nbuf.at[2], near_in.at[2], right)
+        if chained:
+            send(2, nbuf.at[0], near_in.at[0], right)
         arrived(1, fbuf.at[low], far_in.at[1])
         merged(2, low, far_in.at[1], nbuf.at[3])
         send(5, nbuf.at[3], near_in.at[3], left)
-        pump(counts[1])
-        for k in range(4):
-            arrived(2 + k, nbuf.at[k], near_in.at[k])
-            if k == 1:
-                pump(counts[2])
+        slot()
 
         def total(rows, one, two):
             def body(r):
                 at = pl.ds(pl.multiple_of(rows.start + r.start, 32), r.size)
                 branch = pown[3, at, :] + near_in[one, r, :].astype(F32) + near_in[two, r, :].astype(F32)
                 value = source[at, :].astype(F32) + branch
-                if target is None:
-                    for j in range(r.size // SEG):
-                        for b in range(feats // 128):
-                            perm[b, pl.ds(at.start // SEG + j, SEG, stride=steps), :] = value[
-                                j * SEG : (j + 1) * SEG, b * 128 : (b + 1) * 128
-                            ]
-                else:
-                    target[at, :] = value.astype(BF16)
+                target[at, :] = value.astype(BF16)
 
             in_row_steps(half, body, 32)
 
-        total(top, 1, 2)
-        total(low, 0, 3)
+        if chained:
+            gather = gathers[layer + 1]
+            for k in (1, 2):
+                arrived(2 + k, nbuf.at[k], near_in.at[k])
+                if k == 1:
+                    slot()
+            total(top, 1, 2)
+            gather_own(layer + 1, target, 0)
+            gather.begin(0)
+            slot()
+            for k in (0, 3):
+                arrived(2 + k, nbuf.at[k], near_in.at[k])
+                if k == 0:
+                    slot()
+            total(low, 0, 3)
+            gather_own(layer + 1, target, 1)
+            gather.begin(1)
+            gather.begin_squares()
+            in_row_steps(tokens, clear, 32)
+            slot()
+        else:
+            for k in range(4):
+                arrived(2 + k, nbuf.at[k], near_in.at[k])
+                if k == 1:
+                    slot()
+            total(top, 1, 2)
+            total(low, 0, 3)
         for k in range(4):
             across(k).wait_send()
         for k in range(6):
@@ -576,47 +592,45 @@
             parts = [perm[b, pl.ds(first + j, SEG, stride=steps), :] for j in range(rows.size // SEG)]
             base[rows, b * 128 : (b + 1) * 128] = jnp.concatenate(parts, axis=0).astype(BF16)
 
-    def finish(rows):
-        for b in range(feats // 128):
-            out[rows, b * 128 : (b + 1) * 128] = perm[b, rows, :].astype(BF16)
-
     in_row_steps(tokens, spread)
     in_row_steps(tokens, collect, 32)
     gather_own(0, base)
-    greet((("sp", n_sp, sp), ("tp", n_tp, tp)))
-
-    pump(1)
-    gather_begin(0)
+    joined()
+
+    slot()
+    gather = gathers[0]
+    gather.begin(0)
+    gather.begin(1)
+    gather.begin_squares()
     in_row_steps(tokens, clear, 32)
-    gather_end(0, (4, 2, 2))
+    slot()
+    for pair in ((0, 2), (1, 3), (4, 5)):
+        for k in pair:
+            gather.got(k)
+        slot()
+    gather.end()
     column(0)
+    slot()
     for layer in range(layers):
         unit = 2 * layer
-        if layer:
-            net.all(unit)
-            project_all(layer)
-        else:
-            pump(4)
-            for i in (0, -1, 1, 2):
-                for p in range(2):
-                    net.group(unit, p, i)
-                    project(layer, p, i)
-                if i == 0:
-                    pump(3)
+        for i in (0, -1, 1, 2):
+            for p in range(2):
+                slot()
+                net.group(unit, p, i)
+                project(layer, p, i)
         mix(layer)
-        pump(3)
         net.all(unit + 1)
         if layer + 1 < layers:
-            reduce(layer, base, own, (0, 4, 2))
-            gather_own(layer + 1, own)
-            gather_begin(layer + 1)
-            pump(2)
-            in_row_steps(tokens, clear, 32)
-            gather_end(layer + 1, (2, 2, 3))
+            reduce(layer, base, own, True)
+            gather = gathers[layer + 1]
+            for k in (0, 3, 2, 1, 4, 5):
+                gather.got(k)
+                slot()
+            gather.end()
             column(layer + 1)
+            slot()
         else:
-            reduce(layer, own, None, (0, 0, 0))
-            in_row_steps(tokens, finish)
+            reduce(layer, own, out, False)
     for unit in range(2 * layers):
         net.drain(unit)
 
@@ -665,8 +679,8 @@
             dma((3 * layers,)),
             dma((4 * layers,)),
             dma((4 * layers, 16)),
-            dma((13,)),
-            dma((13,)),
+            dma((14,)),
+            dma((14,)),
             dma((layers, n_tp)),
             dma((layers, n_tp)),
             dma((layers, 2)),
@@ -692,9 +706,11 @@
     width = value_proj.shape[2]
     layers = value_proj.shape[0]
     gates = block_gates.reshape(layers, 4, width // 128, 128, 128)
-    return whole_call(
+    stream = whole_call(
         stream_in, norm_gain, value_proj, gate_proj, out_proj, conv_taps, gates, forget_rate, n_sp, n_tp
     )
+    tokens, feats = stream.shape
+    return stream.reshape(tokens // SEG, SEG, feats).transpose(1, 0, 2).reshape(tokens, feats)
 
 
 def solution(mesh):

time: 193 us -> 182 us (0.943)
  Pallas kernels: 191 us -> 180 us
    pallas_call x1, Pallas kernels: 191 us -> 180 us  [whole_call(): pl.pallas_call(functools.partial(whole_kernel, layers, n_sp, n_tp, float(...]
    transpose x0 -> x1, local copies, waits for them, and re-layouts: none -> 1.99 us  [per_device(): stream.reshape(tokens // SEG, SEG, feats).transpose(1, 0, 2)]
where the time goes in v4:
time: 182 us
  Pallas kernels  180 us (99%)
  local copies, waits for them, and re-layouts  1.99 us (1%)
    pallas_call x1, Pallas kernels, whole_call(): pl.pallas_call(functools.partial(whole_kernel, layers, n_sp, n_tp, float(...  180 us

profile of v4, /device:TPU:1, one launch (start us, length us, event | category | flops | bytes accessed | tf_op | source)
XLA Modules:
  0.0 181.7 jit_solution(9877233638458910403)
XLA Ops:
  0.0 179.7 %both_layers.1 = bf16[512,512]{1,0:T(8,128)(2,1)} custom-call(bf16[512,512]{1,0:T(8,128)(2,1)} %stream_ref.1, f32[2,4096]{1,0:T(2,128)} %gain_ref.1, bf16[2,256,512]{2,1,0:T(8,128)(2,1)} %wv_hbm.1, bf16[2,256,512]{2,1,0:T(8,128)(2,1)} %wg_hbm.1, bf16[2,256,512]{2,1,0:T(8,128)(2,1)} %wo_hbm.1, f32[2,4,4096]{2,1,0:T(4,128)} %taps_ref.1, ...), custom_call_target="tpu_custom_call" | custom-call | flops 20000000000 | bytes 8000000 | tf_op jit(solution)/shard_map/both_layers/pallas_call | solution.py:648
  179.7 2.0 %copy.9 = bf16[8,64,512]{2,1,0:T(8,128)(2,1)} copy(bf16[8,64,512]{2,0,1:T(8,128)(2,1)} %bitcast.5) | data formatting | bytes 1048576 | tf_op jit(solution)/shard_map/transpose | solution.py:713

commit v5 on v4

--- a/solution.py
+++ b/solution.py
@@ -14,7 +14,7 @@
 BF16 = jnp.bfloat16
 SEG = 8
 ROWS = 64
-PLAN = ('000', '00', '0', '000', '01', '000', '', '', '', '01', '01', '', '11111', '', '11111', '', '', '', '1', '', '1', '2', '', '3', '2', '', '2', '2', '2', '', '2', '2', '2', '2', '2', '2', '223', '2', '', '', '2', '3', '', '333', '', '', '', '', '33', '3', '3', '', '33', '', '3', '33', '', '', '', '', '', '', '', '')
+PLAN = ('000', '00', '000', '001', '', '0', '', '0', '0010111', '1', '1', '', '1', '', '1111', '', '', '', '', '', '', '1112', '', '', '2', '', '2', '22', '', '22', '22', '2', '22', '23', '', '22', '', '33', '', '', '', '', '', '', '', '3', '', '3', '33333', '', '', '', '', '', '', '33333', '', '', '', '', '', '', '', '')
 
 
 def remote(src, dst, send_sem, recv_sem, dev):
@@ -228,11 +228,11 @@
 
 def whole_kernel(
     layers, n_sp, n_tp, features,
-    stream_ref, gain_ref, wv_hbm, wg_hbm, wo_hbm, taps_ref, gates_ref, rate_ref, out,
+    stream_hbm, gain_hbm, wv_hbm, wg_hbm, wo_hbm, taps_hbm, gates_hbm, rate_hbm, out_hbm,
     wvg, wo, xg, ssg, base, own, perm, acc, mixb, mpad, sil, conv, convb, big, a_f, u_f, a_b, u_b, col,
     halo_p, halo_n, seg, ent, msg, slots,
     psend, precv, fbuf, far_in, nbuf, near_in,
-    ld, gsend, grecv, asend, arecv, ssend, srecv, hsend, hrecv, csend, crecv, ds, dr, rs, rr,
+    stream_ref, gain_ref, taps_ref, gates_ref, rate_ref, ld, ins, outs, gsend, grecv, asend, arecv, ssend, srecv, hsend, hrecv, csend, crecv, ds, dr, rs, rr,
 ):
     sp, tp = lax.axis_index("sp"), lax.axis_index("tp")
     tokens, width = mixb.shape
@@ -244,6 +244,15 @@
     lanes_own = pl.ds(pl.multiple_of(tp * width, width), width)
     right, left = ring.at(1), ring.at(-1)
 
+    inputs = [
+        pltpu.make_async_copy(stream_hbm, stream_ref, ins.at[0]),
+        pltpu.make_async_copy(gain_hbm.at[:, lanes_own], gain_ref, ins.at[1]),
+        pltpu.make_async_copy(taps_hbm.at[:, :, lanes_own], taps_ref, ins.at[2]),
+        pltpu.make_async_copy(gates_hbm, gates_ref, ins.at[3]),
+        pltpu.make_async_copy(rate_hbm.at[:, :, lanes_own], rate_ref, ins.at[4]),
+    ]
+    for copy in inputs:
+        copy.start()
     loads = []
     for layer in range(layers):
         loads.append([
@@ -292,7 +301,7 @@
     ]
 
     def gather_own(layer, source, half=None):
-        gain = gain_ref[layer : layer + 1, lanes_own]
+        gain = gain_ref[layer : layer + 1, :]
         gather_fill(source, gain, xg, ssg.at[layer], tp, half)
 
     def column(layer):
@@ -314,6 +323,9 @@
             mixb[rows, :] = value
             acc[0, rows, :] = value.astype(F32)
 
+        if not layer:
+            for copy in inputs[2:]:
+                copy.wait()
         finish_v(pl.ds(0, 32))
         finish_v(pl.ds(tokens - 32, 32))
         head, tail = mixb.at[pl.ds(0, 16)], mixb.at[pl.ds(tokens - 16, 16)]
@@ -331,7 +343,7 @@
 
         in_row_steps(tokens - 64, finish_v, 32, 32)
         in_row_steps(tokens, finish_g, 32)
-        taps = taps_ref[layer, :, lanes_own]
+        taps = taps_ref[layer]
         maps = [jnp.concatenate([gates_ref[layer, g, b] for g in range(4)], axis=1) for b in range(width // 128)]
         quarter = tokens // 4
 
@@ -373,7 +385,7 @@
         gate_maps(pl.ds(0, quarter))
         gate_maps(pl.ds(3 * quarter, quarter))
         slot()
-        rate_all = -GATE_SCALE * rate_ref[layer, :, lanes_own]
+        rate_all = -GATE_SCALE * rate_ref[layer]
         for b in range(width // 128):
             lanes = pl.ds(b * 128, 128)
             rates = [rate_all[e : e + 1, b * 128 : (b + 1) * 128] for e in range(2)]
@@ -461,6 +473,9 @@
     half = tokens // 2
     top, low = pl.ds(0, half), pl.ds(half, half)
 
+    def result(rows):
+        return pltpu.make_async_copy(base.at[rows], out_hbm.at[rows], outs.at[rows.start // half])
+
     def reduce(layer, source, target, chained):
         order = (2, 1, -1, 0)
 
@@ -574,7 +589,9 @@
                 if k == 1:
                     slot()
             total(top, 1, 2)
+            result(top).start()
             total(low, 0, 3)
+            result(low).start()
         for k in range(4):
             across(k).wait_send()
         for k in range(6):
@@ -592,8 +609,10 @@
             parts = [perm[b, pl.ds(first + j, SEG, stride=steps), :] for j in range(rows.size // SEG)]
             base[rows, b * 128 : (b + 1) * 128] = jnp.concatenate(parts, axis=0).astype(BF16)
 
+    inputs[0].wait()
     in_row_steps(tokens, spread)
     in_row_steps(tokens, collect, 32)
+    inputs[1].wait()
     gather_own(0, base)
     joined()
 
@@ -630,7 +649,9 @@
             column(layer + 1)
             slot()
         else:
-            reduce(layer, own, out, False)
+            reduce(layer, own, base, False)
+            result(top).wait()
+            result(low).wait()
     for unit in range(2 * layers):
         net.drain(unit)
 
@@ -640,7 +661,6 @@
     layers, rows, width = wv.shape
     half = tokens // 2
     blocks = width // 128
-    vmem = pl.BlockSpec(memory_space=pltpu.VMEM)
     hbm = pl.BlockSpec(memory_space=pl.ANY)
     f32 = pltpu.VMEM((tokens, width), F32)
     b16 = pltpu.VMEM((tokens, width), BF16)
@@ -648,8 +668,8 @@
     return pl.pallas_call(
         functools.partial(whole_kernel, layers, n_sp, n_tp, float(gain.shape[1])),
         out_shape=jax.ShapeDtypeStruct((tokens, feats), BF16),
-        in_specs=[vmem, vmem, hbm, hbm, hbm, vmem, vmem, vmem],
-        out_specs=vmem,
+        in_specs=[hbm] * 8,
+        out_specs=hbm,
         scratch_shapes=[
             pltpu.VMEM((layers, 2, n_sp, rows, width), BF16),
             pltpu.VMEM((layers, n_sp, rows, width), BF16),
@@ -676,7 +696,14 @@
             pltpu.VMEM((2, half, feats), BF16),
             pltpu.VMEM((4, half, feats), BF16),
             pltpu.VMEM((4, half, feats), BF16),
+            b16,
+            pltpu.VMEM((layers, feats), F32),
+            pltpu.VMEM((layers, 4, width), F32),
+            pltpu.VMEM(gates.shape, BF16),
+            pltpu.VMEM((layers, 2, width), F32),
             dma((3 * layers,)),
+            dma((5,)),
+            dma((2,)),
             dma((4 * layers,)),
             dma((4 * layers, 16)),
             dma((14,)),

time: 182 us -> 174 us (0.956)
  Pallas kernels: 180 us -> 172 us
    pallas_call x1, Pallas kernels: 180 us -> 172 us  [whole_call(): pl.pallas_call(functools.partial(whole_kernel, layers, n_sp, n_tp, float(...]
where the time goes in v5:
time: 174 us
  Pallas kernels  172 us (99%)
  local copies, waits for them, and re-layouts  1.99 us (1%)
    pallas_call x1, Pallas kernels, whole_call(): pl.pallas_call(functools.partial(whole_kernel, layers, n_sp, n_tp, float(...  172 us

profile of v5, /device:TPU:1, one launch (start us, length us, event | category | flops | bytes accessed | tf_op | source)
XLA Modules:
  0.0 174.0 jit_solution(9772120566567085035)
XLA Ops:
  0.0 172.0 %both_layers.1 = bf16[512,512]{1,0:T(8,128)(2,1)} custom-call(bf16[512,512]{1,0:T(8,128)(2,1)} %stream_hbm.1, f32[2,4096]{1,0:T(2,128)} %gain_hbm.1, bf16[2,256,512]{2,1,0:T(8,128)(2,1)} %wv_hbm.1, bf16[2,256,512]{2,1,0:T(8,128)(2,1)} %wg_hbm.1, bf16[2,256,512]{2,1,0:T(8,128)(2,1)} %wo_hbm.1, f32[2,4,4096]{2,1,0:T(4,128)} %taps_hbm.1, ...), custom_call_target="tpu_custom_call" | custom-call | flops 20000000000 | bytes 8000000 | tf_op jit(solution)/shard_map/both_layers/pallas_call | solution.py:668
  172.0 2.0 %copy.9 = bf16[8,64,512]{2,1,0:T(8,128)(2,1)} copy(bf16[8,64,512]{2,0,1:T(8,128)(2,1)} %bitcast.5) | data formatting | bytes 1048576 | tf_op jit(solution)/shard_map/transpose | solution.py:740

commit v6 on v5

--- a/solution.py
+++ b/solution.py
@@ -12,6 +12,7 @@
 MESH = pl.DeviceIdType.MESH
 F32 = jnp.float32
 BF16 = jnp.bfloat16
+EDGE = 16
 SEG = 8
 ROWS = 64
 PLAN = ('000', '00', '000', '001', '', '0', '', '0', '0010111', '1', '1', '', '1', '', '1111', '', '', '', '', '', '', '1112', '', '', '2', '', '2', '22', '', '22', '22', '2', '22', '23', '', '22', '', '33', '', '', '', '', '', '', '', '3', '', '3', '33333', '', '', '', '', '', '', '33333', '', '', '', '', '', '', '', '')
@@ -36,7 +37,7 @@
 
 
 def drive_square(y):
-    terms = [1.0, -1.0 / 2, 1.0 / 6, -1.0 / 24, 1.0 / 120, -1.0 / 720, 1.0 / 5040, -1.0 / 40320, 1.0 / 362880]
+    terms = [0.999999999543, -0.499999943611, 0.166665528456, -0.0416580188735, 0.00830184073719, -0.00132924407794, 0.000140574729006]
     total = jnp.full_like(y, terms[-1])
     for term in terms[-2::-1]:
         total = total * y + term
@@ -89,11 +90,11 @@
     def __init__(self, ring, xg, ssg, send, recv, ssend, srecv, count):
         self.ring, self.xg, self.ssg, self.count = ring, xg, ssg, count
         self.send, self.recv, self.ssend, self.srecv = send, recv, ssend, srecv
-        half = xg.shape[1] // 2
+        half = (xg.shape[1] - EDGE) // 2
         self.rows = (pl.ds(0, half), pl.ds(half, half))
 
     def push(self, part, k, dev):
-        remote(part, part, self.send.at[k], self.recv.at[k], {"tp": dev}).start()
+        remote(part, part, self.send.at[0], self.recv.at[min(k, 6)], {"tp": dev}).start()
 
     def begin(self, half):
         ring = self.ring
@@ -112,13 +113,13 @@
         ring, ssg = self.ring, self.ssg
         for step in range(1, self.count):
             dev = lax.rem(ring.me + step, self.count)
-            remote(ssg.at[ring.me], ssg.at[ring.me], self.ssend.at[dev], self.srecv.at[ring.me], {"tp": dev}).start()
+            remote(ssg.at[ring.me], ssg.at[ring.me], self.ssend, self.srecv, {"tp": dev}).start()
 
     def got(self, k):
         ring = self.ring
         step, half = {0: (-1, 0), 1: (-1, 1), 2: (1, 1), 3: (1, 0), 4: (2, 0), 5: (2, 1)}[k]
         part = self.xg.at[ring.at(step), self.rows[half]]
-        remote(part, part, self.send.at[k], self.recv.at[k], {"tp": ring.sib}).wait_recv()
+        remote(part, part, self.send.at[0], self.recv.at[k], {"tp": ring.sib}).wait_recv()
         if k == 0:
             self.push(part, 4, ring.at(1))
         if k == 2:
@@ -126,17 +127,14 @@
         self.push(part, 7 + k, ring.sib)
 
     def end(self):
-        ring = self.ring
-        owners = {6: (0, 0), 13: (0, 1), 7: (-1, 0), 8: (-1, 1), 9: (1, 1), 10: (1, 0), 11: (2, 0), 12: (2, 1)}
-        for k, (step, half) in owners.items():
-            part = self.xg.at[ring.at(step, other=True), self.rows[half]]
-            remote(part, part, self.send.at[k], self.recv.at[k], {"tp": ring.sib}).wait()
-        for k in range(6):
-            part = self.xg.at[ring.me, self.rows[0]]
-            remote(part, part, self.send.at[k], self.recv.at[k], {"tp": ring.at(1)}).wait_send()
-        for step in range(1, self.count):
-            dev = lax.rem(ring.me + step, self.count)
-            remote(self.ssg.at[dev], self.ssg.at[dev], self.ssend.at[dev], self.srecv.at[dev], {"tp": dev}).wait()
+        count, dev = self.count, {"tp": self.ring.sib}
+        half = self.rows[0].size
+        came = self.xg.at[:, pl.ds(0, half)]
+        remote(came, came, self.send.at[0], self.recv.at[6], dev).wait_recv()
+        sent = self.xg.at[pl.ds(0, count - 1), pl.ds(0, 2 * half)]
+        remote(sent, sent, self.send.at[0], self.recv.at[6], dev).wait_send()
+        others = self.ssg.at[pl.ds(0, count - 1)]
+        remote(others, others, self.ssend, self.srecv, dev).wait()
 
 
 class Weights:
@@ -229,10 +227,10 @@
 def whole_kernel(
     layers, n_sp, n_tp, features,
     stream_hbm, gain_hbm, wv_hbm, wg_hbm, wo_hbm, taps_hbm, gates_hbm, rate_hbm, out_hbm,
-    wvg, wo, xg, ssg, base, own, perm, acc, mixb, mpad, sil, conv, convb, big, a_f, u_f, a_b, u_b, col,
-    halo_p, halo_n, seg, ent, msg, slots,
+    wvg, wo, xg, ssg, edge, near, tok, base, own, perm, acc, mixb, mpad, sil, conv, convb, big, a_f, u_f, a_b, u_b, col,
+    seg, ent, msg, slots,
     psend, precv, fbuf, far_in, nbuf, near_in,
-    stream_ref, gain_ref, taps_ref, gates_ref, rate_ref, ld, ins, outs, gsend, grecv, asend, arecv, ssend, srecv, hsend, hrecv, csend, crecv, ds, dr, rs, rr,
+    stream_ref, gain_ref, taps_ref, gates_ref, rate_ref, ld, ins, outs, gsend, grecv, asend, arecv, ssend, srecv, hsend, hrecv, esend, erecv, csend, crecv, ds, dr, rs, rr,
 ):
     sp, tp = lax.axis_index("sp"), lax.axis_index("tp")
     tokens, width = mixb.shape
@@ -246,7 +244,7 @@
 
     inputs = [
         pltpu.make_async_copy(stream_hbm, stream_ref, ins.at[0]),
-        pltpu.make_async_copy(gain_hbm.at[:, lanes_own], gain_ref, ins.at[1]),
+        pltpu.make_async_copy(gain_hbm, gain_ref, ins.at[1]),
         pltpu.make_async_copy(taps_hbm.at[:, :, lanes_own], taps_ref, ins.at[2]),
         pltpu.make_async_copy(gates_hbm, gates_ref, ins.at[3]),
         pltpu.make_async_copy(rate_hbm.at[:, :, lanes_own], rate_ref, ins.at[4]),
@@ -287,13 +285,62 @@
             first = lax.rem(net.z + i + net.side, net.side) * 2
             terms = [
                 jnp.dot(
-                    xg[first + j],
+                    xg[first + j, 0:tokens, :],
                     wvg[layer, p, pl.ds(2 * (first + j), 2)].reshape(feats, width),
                     preferred_element_type=F32,
                 )
                 for j in range(2)
             ]
-        acc[p] += functools.reduce(jnp.add, terms)
+        total = functools.reduce(jnp.add, terms)
+        acc[p, 0 : total.shape[0], :] += total
+
+    def edge_send(layer, source):
+        ends = (source[0:16, :].astype(F32), source[tokens - 16 : tokens, :].astype(F32))
+        spots = ((0, 0), (1, 7), (1, 15))
+        lines = [
+            ends[side][row : row + 1, b * 128 : (b + 1) * 128] for side, row in spots for b in range(feats // 128)
+        ]
+        tok[layer] = jnp.concatenate(lines + [jnp.zeros((16 - len(lines), 128), F32)], axis=0).astype(BF16)
+        for k in range(2):
+            edge_copy(layer, k).start()
+
+    def edge_copy(layer, k):
+        place = lax.rem(sp + (1 if k == 0 else n_sp - 1), n_sp)
+        return remote(tok.at[layer], near.at[layer, k], hsend.at[layer, k], hrecv.at[layer, k], {"sp": place})
+
+    def edge_share(layer):
+        for k in range(2):
+            edge_copy(layer, k).wait()
+        rows = lax.broadcasted_iota(jnp.int32, (16, 128), 0)
+        after = jnp.where(sp < n_sp - 1, near[layer, 1].astype(F32), 0.0)
+        before = jnp.where(sp > 0, near[layer, 0].astype(F32), 0.0)
+        edge[layer, tp] = jnp.where(rows < 4, after, before).astype(BF16)
+        for step in range(1, n_tp):
+            dev = lax.rem(tp + step, n_tp)
+            remote(
+                edge.at[layer, tp], edge.at[layer, tp], esend.at[layer], erecv.at[layer], {"tp": dev}
+            ).start()
+
+    def edge_rows(layer):
+        whole = edge.at[layer, pl.ds(0, n_tp - 1)]
+        remote(whole, whole, esend.at[layer], erecv.at[layer], {"tp": ring.sib}).wait()
+        squares = jnp.zeros((16, 128), F32)
+        for block in range(n_tp):
+            values = edge[layer, block].astype(F32)
+            squares = squares + values * values
+            lines = []
+            for r in range(3):
+                parts = [values[4 * r + b : 4 * r + b + 1, :] for b in range(feats // 128)]
+                lines.append(jnp.concatenate(parts, axis=1))
+            gain = gain_ref[layer : layer + 1, pl.ds(block * feats, feats)]
+            rows = jnp.concatenate(lines, axis=0) * gain
+            filled = jnp.concatenate([rows, jnp.zeros((EDGE - 3, feats), F32)], axis=0)
+            xg[block, pl.ds(tokens, EDGE), :] = filled.astype(BF16)
+        sums = jnp.sum(squares, axis=1, keepdims=True)
+        return [
+            lax.rsqrt(jnp.sum(sums[4 * r : 4 * r + 4, :], axis=0, keepdims=True) / features + NORM_EPS)
+            for r in range(3)
+        ]
 
     gathers = [
         Gather(ring, xg, ssg.at[layer], asend, arecv, ssend.at[layer], srecv.at[layer], n_tp)
@@ -301,7 +348,7 @@
     ]
 
     def gather_own(layer, source, half=None):
-        gain = gain_ref[layer : layer + 1, :]
+        gain = gain_ref[layer : layer + 1, lanes_own]
         gather_fill(source, gain, xg, ssg.at[layer], tp, half)
 
     def column(layer):
@@ -316,7 +363,11 @@
         acc[0, rows, :] = zero
         acc[1, rows, :] = zero
 
-    def mix(layer):
+    def clear_all():
+        in_row_steps(tokens, clear, 32)
+        acc[0, pl.ds(tokens, EDGE), :] = jnp.zeros((EDGE, width), F32)
+
+    def mix(layer, scales):
         def finish_v(rows):
             wide = jnp.concatenate([col[rows, :]] * (width // 128), axis=1)
             value = (acc[0, rows, :] * wide).astype(BF16)
@@ -326,14 +377,6 @@
         if not layer:
             for copy in inputs[2:]:
                 copy.wait()
-        finish_v(pl.ds(0, 32))
-        finish_v(pl.ds(tokens - 32, 32))
-        head, tail = mixb.at[pl.ds(0, 16)], mixb.at[pl.ds(tokens - 16, 16)]
-        hs, hr = hsend.at[layer], hrecv.at[layer]
-        to_next = remote(tail, halo_p.at[layer], hs.at[0], hr.at[0], {"sp": lax.rem(sp + 1, n_sp)})
-        to_prev = remote(head, halo_n.at[layer], hs.at[1], hr.at[1], {"sp": lax.rem(sp + n_sp - 1, n_sp)})
-        to_next.start()
-        to_prev.start()
 
         def finish_g(rows):
             wide = jnp.concatenate([col[rows, :]] * (width // 128), axis=1)
@@ -341,11 +384,24 @@
             sil[rows, :] = gate * sigmoid(gate)
             mpad[pl.ds(aligned(rows.start + 16, 16), rows.size), :] = acc[0, rows, :]
 
-        in_row_steps(tokens - 64, finish_v, 32, 32)
+        in_row_steps(tokens, finish_v, 32)
         in_row_steps(tokens, finish_g, 32)
+        slot()
+        edges = [
+            (acc[0, tokens + r : tokens + r + 1, :] * scales[r]).astype(BF16).astype(F32) for r in range(3)
+        ]
+        sub = lax.broadcasted_iota(jnp.int32, (SEG, width), 0)
+        for k in range(2):
+            blk = acc[0, pl.ds(tokens - 16 + 8 * k, 8), :]
+            mpad[pl.ds(8 * k, 8), :] = jnp.where(
+                sub == 0, jnp.broadcast_to(edges[1 + k], (SEG, width)), pltpu.roll(blk, 1, 0)
+            )
+        blk = acc[0, pl.ds(0, 8), :]
+        mpad[pl.ds(tokens + 16, 8), :] = jnp.where(
+            sub == SEG - 1, jnp.broadcast_to(edges[0], (SEG, width)), pltpu.roll(blk, SEG - 1, 0)
+        )
         taps = taps_ref[layer]
         maps = [jnp.concatenate([gates_ref[layer, g, b] for g in range(4)], axis=1) for b in range(width // 128)]
-        quarter = tokens // 4
 
         def gate_maps(rows):
             for b in range(width // 128):
@@ -360,30 +416,9 @@
             conv[rows, :] = value
             convb[rows, :] = value.astype(BF16)
 
-        in_row_steps(tokens - 64, convolve, 32, 32)
-        gate_maps(pl.ds(quarter, 2 * quarter))
+        in_row_steps(tokens, convolve, 32)
         slot()
-        to_next.wait()
-        to_prev.wait()
-        sub = lax.broadcasted_iota(jnp.int32, (SEG, width), 0)
-        before = halo_p[layer].astype(F32)
-        after = halo_n[layer].astype(F32)
-        for k in range(2):
-            edge = jnp.where(sp > 0, before[8 * k + 7 : 8 * k + 8, :], 0.0)
-            blk = acc[0, pl.ds(tokens - 16 + 8 * k, 8), :]
-            mpad[pl.ds(8 * k, 8), :] = jnp.where(
-                sub == 0, jnp.broadcast_to(edge, (SEG, width)), pltpu.roll(blk, 1, 0)
-            )
-        edge = jnp.where(sp < n_sp - 1, after[0:1, :], 0.0)
-        blk = acc[0, pl.ds(0, 8), :]
-        mpad[pl.ds(tokens + 16, 8), :] = jnp.where(
-            sub == SEG - 1, jnp.broadcast_to(edge, (SEG, width)), pltpu.roll(blk, SEG - 1, 0)
-        )
-        convolve(pl.ds(0, 32))
-        convolve(pl.ds(tokens - 32, 32))
-        slot()
-        gate_maps(pl.ds(0, quarter))
-        gate_maps(pl.ds(3 * quarter, quarter))
+        gate_maps(pl.ds(0, tokens))
         slot()
         rate_all = -GATE_SCALE * rate_ref[layer]
         for b in range(width // 128):
@@ -435,12 +470,11 @@
         for step in range(1, n_sp):
             dev = lax.rem(sp + step, n_sp)
             side = jnp.where(dev > sp, 0, 1)
-            remote(msg.at[layer, side], slots.at[layer, sp], cs.at[dev], cr.at[sp], {"sp": dev}).start()
+            remote(msg.at[layer, side], slots.at[layer, sp], cs, cr, {"sp": dev}).start()
         slots[layer, sp] = jnp.zeros((8, 128), F32)
         slot()
-        for step in range(1, n_sp):
-            dev = lax.rem(sp + step, n_sp)
-            remote(msg.at[layer, 0], slots.at[layer, dev], cs.at[dev], cr.at[dev], {"sp": dev}).wait()
+        others = slots.at[layer, pl.ds(0, n_sp - 1)]
+        remote(others, others, cs, cr, {"sp": lax.rem(sp + 1, n_sp)}).wait()
         for e, (k, order) in enumerate(sides):
             carry = jnp.zeros((4, 128), F32)
             for q in range(n_sp) if e == 0 else range(n_sp - 1, -1, -1):
@@ -490,10 +524,10 @@
             return terms
 
         def across(k):
-            return remote(psend.at[k], precv.at[k], ds.at[k], dr.at[k], {"tp": ring.sib})
+            return remote(psend.at[k], precv.at[k], ds.at[0], dr.at[k], {"tp": ring.sib})
 
         def send(k, src, dst, dev):
-            remote(src, dst, rs.at[k], rr.at[k], {"tp": dev}).start()
+            remote(src, dst, rs.at[0], rr.at[k], {"tp": dev}).start()
 
         def paired(k, rows, into=None):
             def body(r):
@@ -535,7 +569,7 @@
         slot()
 
         def arrived(k, src, dst):
-            remote(src, dst, rs.at[k], rr.at[k], {"tp": right}).wait_recv()
+            remote(src, dst, rs.at[0], rr.at[k], {"tp": right}).wait_recv()
 
         def merged(k, rows, src, into):
             def body(r):
@@ -581,7 +615,8 @@
             gather_own(layer + 1, target, 1)
             gather.begin(1)
             gather.begin_squares()
-            in_row_steps(tokens, clear, 32)
+            edge_send(layer + 1, target)
+            clear_all()
             slot()
         else:
             for k in range(4):
@@ -592,10 +627,9 @@
             result(top).start()
             total(low, 0, 3)
             result(low).start()
-        for k in range(4):
-            across(k).wait_send()
-        for k in range(6):
-            remote(nbuf.at[0], near_in.at[0], rs.at[k], rr.at[k], {"tp": right}).wait_send()
+        remote(psend, precv, ds.at[0], dr.at[0], {"tp": ring.sib}).wait_send()
+        six = psend.at[pl.ds(0, 3)]
+        remote(six, six, rs.at[0], rr.at[0], {"tp": right}).wait_send()
 
     steps = tokens // SEG
 
@@ -621,13 +655,17 @@
     gather.begin(0)
     gather.begin(1)
     gather.begin_squares()
-    in_row_steps(tokens, clear, 32)
+    edge_send(0, base)
+    clear_all()
     slot()
     for pair in ((0, 2), (1, 3), (4, 5)):
         for k in pair:
             gather.got(k)
+        if pair[0] == 0:
+            edge_share(0)
         slot()
     gather.end()
+    scales = edge_rows(0)
     column(0)
     slot()
     for layer in range(layers):
@@ -637,15 +675,18 @@
                 slot()
                 net.group(unit, p, i)
                 project(layer, p, i)
-        mix(layer)
+        mix(layer, scales)
         net.all(unit + 1)
         if layer + 1 < layers:
             reduce(layer, base, own, True)
             gather = gathers[layer + 1]
             for k in (0, 3, 2, 1, 4, 5):
                 gather.got(k)
+                if k == 2:
+                    edge_share(layer + 1)
                 slot()
             gather.end()
+            scales = edge_rows(layer + 1)
             column(layer + 1)
             slot()
         else:
@@ -673,19 +714,20 @@
         scratch_shapes=[
             pltpu.VMEM((layers, 2, n_sp, rows, width), BF16),
             pltpu.VMEM((layers, n_sp, rows, width), BF16),
-            pltpu.VMEM((n_tp, tokens, feats), BF16),
+            pltpu.VMEM((n_tp, tokens + EDGE, feats), BF16),
             pltpu.VMEM((layers, n_tp, 8, tokens), F32),
+            pltpu.VMEM((layers, n_tp, 16, 128), BF16),
+            pltpu.VMEM((layers, 2, 16, 128), BF16),
+            pltpu.VMEM((layers, 16, 128), BF16),
             b16, b16,
             pltpu.VMEM((feats // 128, tokens, 128), F32),
-            pltpu.VMEM((2, tokens, width), F32),
+            pltpu.VMEM((2, tokens + EDGE, width), F32),
             b16,
             pltpu.VMEM((tokens + 24, width), F32),
             f32, f32, b16,
             pltpu.VMEM((4, tokens, 512), F32),
             f32, f32, f32, f32,
             pltpu.VMEM((tokens, 128), F32),
-            pltpu.VMEM((layers, 16, width), BF16),
-            pltpu.VMEM((layers, 16, width), BF16),
             pltpu.VMEM((4, SEG, width), F32),
             pltpu.VMEM((2, SEG, width), F32),
             pltpu.VMEM((layers, 2, 8, 128), F32),
@@ -697,7 +739,7 @@
             pltpu.VMEM((4, half, feats), BF16),
             pltpu.VMEM((4, half, feats), BF16),
             b16,
-            pltpu.VMEM((layers, feats), F32),
+            pltpu.VMEM(gain.shape, F32),
             pltpu.VMEM((layers, 4, width), F32),
             pltpu.VMEM(gates.shape, BF16),
             pltpu.VMEM((layers, 2, width), F32),
@@ -706,17 +748,19 @@
             dma((2,)),
             dma((4 * layers,)),
             dma((4 * layers, 16)),
-            dma((14,)),
-            dma((14,)),
-            dma((layers, n_tp)),
-            dma((layers, n_tp)),
+            dma((1,)),
+            dma((7,)),
+            dma((layers,)),
+            dma((layers,)),
             dma((layers, 2)),
             dma((layers, 2)),
-            dma((layers, n_sp)),
-            dma((layers, n_sp)),
+            dma((layers,)),
+            dma((layers,)),
+            dma((layers,)),
+            dma((layers,)),
+            dma((1,)),
             dma((4,)),
-            dma((4,)),
-            dma((6,)),
+            dma((1,)),
             dma((6,)),
         ],
         compiler_params=pltpu.CompilerParams(

time: 174 us -> 169 us (0.971)
  Pallas kernels: 172 us -> 167 us
    pallas_call x1, Pallas kernels: 172 us -> 167 us  [whole_call(): pl.pallas_call(functools.partial(whole_kernel, layers, n_sp, n_tp, float(...]
where the time goes in v6:
time: 169 us
  Pallas kernels  167 us (99%)
  local copies, waits for them, and re-layouts  1.99 us (1%)
    pallas_call x1, Pallas kernels, whole_call(): pl.pallas_call(functools.partial(whole_kernel, layers, n_sp, n_tp, float(...  167 us

profile of v6, /device:TPU:1, one launch (start us, length us, event | category | flops | bytes accessed | tf_op | source)
XLA Modules:
  0.0 168.8 jit_solution(2203370577292407726)
XLA Ops:
  0.0 166.8 %both_layers.1 = bf16[512,512]{1,0:T(8,128)(2,1)} custom-call(bf16[512,512]{1,0:T(8,128)(2,1)} %stream_hbm.1, f32[2,4096]{1,0:T(2,128)} %gain_hbm.1, bf16[2,256,512]{2,1,0:T(8,128)(2,1)} %wv_hbm.1, bf16[2,256,512]{2,1,0:T(8,128)(2,1)} %wg_hbm.1, bf16[2,256,512]{2,1,0:T(8,128)(2,1)} %wo_hbm.1, f32[2,4,4096]{2,1,0:T(4,128)} %taps_hbm.1, ...), custom_call_target="tpu_custom_call" | custom-call | flops 20000000000 | bytes 8000000 | tf_op jit(solution)/shard_map/both_layers/pallas_call | solution.py:709
  166.8 2.0 %copy.9 = bf16[8,64,512]{2,1,0:T(8,128)(2,1)} copy(bf16[8,64,512]{2,0,1:T(8,128)(2,1)} %bitcast.5) | data formatting | bytes 1048576 | tf_op jit(solution)/shard_map/transpose | solution.py:784

commit v7 on v6

--- a/solution.py
+++ b/solution.py
@@ -15,7 +15,7 @@
 EDGE = 16
 SEG = 8
 ROWS = 64
-PLAN = ('000', '00', '000', '001', '', '0', '', '0', '0010111', '1', '1', '', '1', '', '1111', '', '', '', '', '', '', '1112', '', '', '2', '', '2', '22', '', '22', '22', '2', '22', '23', '', '22', '', '33', '', '', '', '', '', '', '', '3', '', '3', '33333', '', '', '', '', '', '', '33333', '', '', '', '', '', '', '', '')
+PLAN = ('0', '00', '00', '00', '01', '00', '00', '001', '1011', '1', '1', '', '1', '1', '', '', '', '', '11', '', '', '11112', '', '', '2', '2', '2', '2', '22', '', '2', '2', '222', '2', '3', '22', '', '3', '3', '', '', '', '', '', '33', '', '', '', '333', '3', '', '', '3', '', '', '33', '', '33', '3', '', '', '', '')
 
 
 def remote(src, dst, send_sem, recv_sem, dev):
@@ -510,126 +510,183 @@
     def result(rows):
         return pltpu.make_async_copy(base.at[rows], out_hbm.at[rows], outs.at[rows.start // half])
 
-    def reduce(layer, source, target, chained):
+    class Reduce:
         order = (2, 1, -1, 0)
 
-        def product(k, other):
-            block = ring.at(order[k], other=other)
-            terms = [
-                lax.dot_general(
-                    mixb[...], wo[layer, 2 * block + part], (((1,), (1,)), ((), ())), preferred_element_type=F32
-                )
-                for part in range(2)
-            ]
-            return terms
-
-        def across(k):
-            return remote(psend.at[k], precv.at[k], ds.at[0], dr.at[k], {"tp": ring.sib})
-
-        def send(k, src, dst, dev):
-            remote(src, dst, rs.at[0], rr.at[k], {"tp": dev}).start()
-
-        def paired(k, rows, into=None):
+        def __init__(self, layer, first, count, shard):
+            self.layer, self.first, self.parts, self.shard = layer, first, range(first, first + count), shard
+            self.sel = pl.ds(first, count)
+
+        def product(self, k, other, part):
+            return lax.dot_general(
+                mixb[...],
+                wo[self.layer, self.shard(self.order[k], other, part)],
+                (((1,), (1,)), ((), ())),
+                preferred_element_type=F32,
+            )
+
+        def across(self, k):
+            return remote(
+                psend.at[k, self.sel], precv.at[k, self.sel], ds.at[0], dr.at[k, self.first], {"tp": ring.sib}
+            )
+
+        def send(self, k, src, dst, dev):
+            remote(src, dst, rs.at[0], rr.at[k, self.first], {"tp": dev}).start()
+
+        def arrived(self, k, dst):
+            remote(dst, dst, rs.at[0], rr.at[k, self.first], {"tp": right}).wait_recv()
+
+        def paired(self, k, rows, into=None):
             def body(r):
                 at = pl.ds(pl.multiple_of(rows.start + r.start, 32), r.size)
-                value = pown[k, at, :] + precv[k, at, :].astype(F32)
-                if into is None:
-                    pown[k, at, :] = value
-                else:
-                    into[at if into.shape[0] == tokens else r, :] = value.astype(BF16)
+                for part in self.parts:
+                    lanes = pl.ds(part * 256, 256)
+                    value = pown[k, at, lanes] + precv[k, part, at, :].astype(F32)
+                    if into is None:
+                        pown[k, at, lanes] = value
+                    elif into is fbuf:
+                        fbuf[part, at, :] = value.astype(BF16)
+                    else:
+                        nbuf[into, part, r, :] = value.astype(BF16)
 
             in_row_steps(rows.size, body, 32)
 
-        for k in range(4):
-            for part, term in enumerate(product(k, True)):
-                psend[k, :, part * 256 : (part + 1) * 256] = term.astype(BF16)
-            across(k).start()
-            for part, term in enumerate(product(k, False)):
-                pown[k, :, part * 256 : (part + 1) * 256] = term
-            if k == 1:
-                across(0).wait_recv()
-                paired(0, top, fbuf)
-                send(0, fbuf.at[top], far_in.at[0], right)
-                paired(0, low, fbuf)
-                send(1, fbuf.at[low], far_in.at[1], left)
-            if k == 2:
-                across(1).wait_recv()
-                paired(1, low, nbuf.at[0])
-                if not chained:
-                    send(2, nbuf.at[0], near_in.at[0], right)
-                paired(1, top)
-            if k == 3:
-                across(2).wait_recv()
-                paired(2, top, nbuf.at[1])
-                send(3, nbuf.at[1], near_in.at[1], left)
-                paired(2, low)
-            slot()
-        across(3).wait_recv()
-        paired(3, pl.ds(0, tokens))
-        slot()
-
-        def arrived(k, src, dst):
-            remote(src, dst, rs.at[0], rr.at[k], {"tp": right}).wait_recv()
-
-        def merged(k, rows, src, into):
+        def near(self, k, dev):
+            self.send(2 + k, nbuf.at[k, self.sel], near_in.at[k, self.sel], dev)
+
+        def opening(self, chained):
+            for k in range(4):
+                for part in self.parts:
+                    psend[k, part] = self.product(k, True, part).astype(BF16)
+                self.across(k).start()
+                for part in self.parts:
+                    pown[k, :, part * 256 : (part + 1) * 256] = self.product(k, False, part)
+                if k == 1:
+                    self.across(0).wait_recv()
+                    self.paired(0, top, fbuf)
+                    self.send(0, fbuf.at[self.sel, top], far_in.at[0, self.sel], right)
+                    self.paired(0, low, fbuf)
+                    self.send(1, fbuf.at[self.sel, low], far_in.at[1, self.sel], left)
+                if k == 2:
+                    self.across(1).wait_recv()
+                    self.paired(1, low, 0)
+                    if not chained:
+                        self.near(0, right)
+                    self.paired(1, top)
+                if k == 3:
+                    self.across(2).wait_recv()
+                    self.paired(2, top, 1)
+                    self.near(1, left)
+                    self.paired(2, low)
+                if chained or not self.first:
+                    slot()
+            self.across(3).wait_recv()
+            self.paired(3, pl.ds(0, tokens))
+
+        def merge(self, k, rows, side):
+            self.arrived(side, far_in.at[side, self.sel])
+
             def body(r):
                 at = pl.ds(pl.multiple_of(rows.start + r.start, 32), r.size)
-                into[r, :] = (pown[k, at, :] + src[r, :].astype(F32)).astype(BF16)
+                for part in self.parts:
+                    value = pown[k, at, pl.ds(part * 256, 256)] + far_in[side, part, r, :].astype(F32)
+                    nbuf[2 + side, part, r, :] = value.astype(BF16)
 
             in_row_steps(half, body, 32)
-
-        arrived(0, fbuf.at[top], far_in.at[0])
-        merged(1, top, far_in.at[0], nbuf.at[2])
-        send(4, nbuf.at[2], near_in.at[2], right)
-        if chained:
-            send(2, nbuf.at[0], near_in.at[0], right)
-        arrived(1, fbuf.at[low], far_in.at[1])
-        merged(2, low, far_in.at[1], nbuf.at[3])
-        send(5, nbuf.at[3], near_in.at[3], left)
-        slot()
-
-        def total(rows, one, two):
+            self.near(2 + side, left if side else right)
+
+        def merges(self, chained):
+            self.merge(1, top, 0)
+            if chained:
+                self.near(0, right)
+            self.merge(2, low, 1)
+
+        def got(self, k):
+            self.arrived(2 + k, near_in.at[k, self.sel])
+
+        def total(self, rows, one, two, source, target, column=None):
             def body(r):
                 at = pl.ds(pl.multiple_of(rows.start + r.start, 32), r.size)
-                branch = pown[3, at, :] + near_in[one, r, :].astype(F32) + near_in[two, r, :].astype(F32)
-                value = source[at, :].astype(F32) + branch
-                target[at, :] = value.astype(BF16)
+                for part in self.parts:
+                    lanes = pl.ds(part * 256, 256)
+                    branch = pown[3, at, lanes] + near_in[one, part, r, :].astype(F32)
+                    branch = branch + near_in[two, part, r, :].astype(F32)
+                    spot = lanes if column is None else column
+                    target[at, spot] = (source[at, spot].astype(F32) + branch).astype(BF16)
 
             in_row_steps(half, body, 32)
 
-        if chained:
-            gather = gathers[layer + 1]
-            for k in (1, 2):
-                arrived(2 + k, nbuf.at[k], near_in.at[k])
-                if k == 1:
-                    slot()
-            total(top, 1, 2)
-            gather_own(layer + 1, target, 0)
-            gather.begin(0)
-            slot()
-            for k in (0, 3):
-                arrived(2 + k, nbuf.at[k], near_in.at[k])
-                if k == 0:
-                    slot()
-            total(low, 0, 3)
-            gather_own(layer + 1, target, 1)
-            gather.begin(1)
-            gather.begin_squares()
-            edge_send(layer + 1, target)
-            clear_all()
-            slot()
-        else:
-            for k in range(4):
-                arrived(2 + k, nbuf.at[k], near_in.at[k])
-                if k == 1:
-                    slot()
-            total(top, 1, 2)
-            result(top).start()
-            total(low, 0, 3)
-            result(low).start()
-        remote(psend, precv, ds.at[0], dr.at[0], {"tp": ring.sib}).wait_send()
+    def reduce_done():
+        remote(psend, precv, ds.at[0], dr.at[0, 0], {"tp": ring.sib}).wait_send()
         six = psend.at[pl.ds(0, 3)]
-        remote(six, six, rs.at[0], rr.at[0], {"tp": right}).wait_send()
+        remote(six, six, rs.at[0], rr.at[0, 0], {"tp": right}).wait_send()
+
+    def reduce_chained(layer, source, target):
+        work = Reduce(layer, 0, 2, lambda step, other, part: 2 * ring.at(step, other=other) + part)
+        work.opening(True)
+        slot()
+        work.merges(True)
+        slot()
+        gather = gathers[layer + 1]
+        work.got(1)
+        slot()
+        work.got(2)
+        work.total(top, 1, 2, source, target)
+        gather_own(layer + 1, target, 0)
+        gather.begin(0)
+        slot()
+        work.got(0)
+        slot()
+        work.got(3)
+        work.total(low, 0, 3, source, target)
+        gather_own(layer + 1, target, 1)
+        gather.begin(1)
+        gather.begin_squares()
+        edge_send(layer + 1, target)
+        clear_all()
+        slot()
+        reduce_done()
+
+    def reduce_last(layer, source, target):
+        unit = 2 * layer + 1
+
+        def stage(first, near_y, far_y):
+            ya, yb = (lax.rem(net.y + d + net.side, net.side) for d in (near_y, far_y))
+            mine = jnp.where(ya // 2 == ring.c, ya, yb)
+            theirs = jnp.where(ya // 2 == ring.c, yb, ya)
+
+            def shard(step, other, part):
+                z = lax.rem(ring.x + step + ring.chips, ring.chips)
+                return z * net.side + (theirs if other else mine)
+
+            column = pl.ds(pl.multiple_of(lax.rem(mine, 2) * 256, 256), 256)
+            return Reduce(layer, first, 1, shard), column
+
+        one, one_column = stage(0, 1, -1)
+        two, two_column = stage(1, 0, 2)
+        for i in (-1, 1):
+            net.group(unit, 0, i)
+        for i in (0, -1, 1, 2):
+            for j in (-1, 1):
+                net.arrive(unit, 1, i, j)
+        one.opening(False)
+        slot()
+        one.merges(False)
+        slot()
+        net.all(unit)
+        two.opening(False)
+        for k in range(4):
+            one.got(k)
+        one.total(top, 1, 2, source, target, one_column)
+        one.total(low, 0, 3, source, target, one_column)
+        two.merges(False)
+        for k in range(4):
+            two.got(k)
+        two.total(top, 1, 2, source, target, two_column)
+        result(top).start()
+        two.total(low, 0, 3, source, target, two_column)
+        result(low).start()
+        reduce_done()
 
     steps = tokens // SEG
 
@@ -676,9 +733,9 @@
                 net.group(unit, p, i)
                 project(layer, p, i)
         mix(layer, scales)
-        net.all(unit + 1)
         if layer + 1 < layers:
-            reduce(layer, base, own, True)
+            net.all(unit + 1)
+            reduce_chained(layer, base, own)
             gather = gathers[layer + 1]
             for k in (0, 3, 2, 1, 4, 5):
                 gather.got(k)
@@ -690,7 +747,7 @@
             column(layer + 1)
             slot()
         else:
-            reduce(layer, own, base, False)
+            reduce_last(layer, own, base)
             result(top).wait()
             result(low).wait()
     for unit in range(2 * layers):
@@ -732,12 +789,12 @@
             pltpu.VMEM((2, SEG, width), F32),
             pltpu.VMEM((layers, 2, 8, 128), F32),
             pltpu.VMEM((layers, n_sp, 8, 128), F32),
-            pltpu.VMEM((4, tokens, feats), BF16),
-            pltpu.VMEM((4, tokens, feats), BF16),
-            pltpu.VMEM((tokens, feats), BF16),
-            pltpu.VMEM((2, half, feats), BF16),
-            pltpu.VMEM((4, half, feats), BF16),
-            pltpu.VMEM((4, half, feats), BF16),
+            pltpu.VMEM((4, 2, tokens, feats // 2), BF16),
+            pltpu.VMEM((4, 2, tokens, feats // 2), BF16),
+            pltpu.VMEM((2, tokens, feats // 2), BF16),
+            pltpu.VMEM((2, 2, half, feats // 2), BF16),
+            pltpu.VMEM((4, 2, half, feats // 2), BF16),
+            pltpu.VMEM((4, 2, half, feats // 2), BF16),
             b16,
             pltpu.VMEM(gain.shape, F32),
             pltpu.VMEM((layers, 4, width), F32),
@@ -759,9 +816,9 @@
             dma((layers,)),
             dma((layers,)),
             dma((1,)),
-            dma((4,)),
+            dma((4, 2)),
             dma((1,)),
-            dma((6,)),
+            dma((6, 2)),
         ],
         compiler_params=pltpu.CompilerParams(
             collective_id=0, has_side_effects=True, vmem_limit_bytes=63_000_000

time: 169 us -> 166 us (0.982)
  Pallas kernels: 167 us -> 164 us
    pallas_call x1, Pallas kernels: 167 us -> 164 us  [whole_call(): pl.pallas_call(functools.partial(whole_kernel, layers, n_sp, n_tp, float(...]
where the time goes in v7:
time: 166 us
  Pallas kernels  164 us (99%)
  local copies, waits for them, and re-layouts  1.99 us (1%)
    pallas_call x1, Pallas kernels, whole_call(): pl.pallas_call(functools.partial(whole_kernel, layers, n_sp, n_tp, float(...  164 us

profile of v7, /device:TPU:1, one launch (start us, length us, event | category | flops | bytes accessed | tf_op | source)
XLA Modules:
  0.0 165.8 jit_solution(17688891246384916551)
XLA Ops:
  0.0 163.8 %both_layers.1 = bf16[512,512]{1,0:T(8,128)(2,1)} custom-call(bf16[512,512]{1,0:T(8,128)(2,1)} %stream_hbm.1, f32[2,4096]{1,0:T(2,128)} %gain_hbm.1, bf16[2,256,512]{2,1,0:T(8,128)(2,1)} %wv_hbm.1, bf16[2,256,512]{2,1,0:T(8,128)(2,1)} %wg_hbm.1, bf16[2,256,512]{2,1,0:T(8,128)(2,1)} %wo_hbm.1, f32[2,4,4096]{2,1,0:T(4,128)} %taps_hbm.1, ...), custom_call_target="tpu_custom_call" | custom-call | flops 20000000000 | bytes 8000000 | tf_op jit(solution)/shard_map/both_layers/pallas_call | solution.py:766
  163.8 2.0 %copy.9 = bf16[8,64,512]{2,1,0:T(8,128)(2,1)} copy(bf16[8,64,512]{2,0,1:T(8,128)(2,1)} %bitcast.5) | data formatting | bytes 1048576 | tf_op jit(solution)/shard_map/transpose | solution.py:841

commit v8 on v7

--- a/solution.py
+++ b/solution.py
@@ -347,6 +347,23 @@
         for layer in range(layers)
     ]
 
+    def project_all(layer, p):
+        rows = pl.ds(0, tokens + EDGE if p == 0 else tokens)
+
+        def four(first):
+            terms = [
+                jnp.dot(
+                    xg[block, rows, :],
+                    wvg[layer, p, 2 * block : 2 * block + 2].reshape(feats, width),
+                    preferred_element_type=F32,
+                )
+                for block in range(first, first + 4)
+            ]
+            return functools.reduce(jnp.add, terms)
+
+        acc[p, rows, :] = four(0)
+        acc[p, rows, :] += four(4)
+
     def gather_own(layer, source, half=None):
         gain = gain_ref[layer : layer + 1, lanes_own]
         gather_fill(source, gain, xg, ssg.at[layer], tp, half)
@@ -556,11 +573,13 @@
 
         def opening(self, chained):
             for k in range(4):
-                for part in self.parts:
-                    psend[k, part] = self.product(k, True, part).astype(BF16)
+                others = [self.product(k, True, part) for part in self.parts]
+                kept = [self.product(k, False, part) for part in self.parts]
+                for part, term in zip(self.parts, others):
+                    psend[k, part] = term.astype(BF16)
+                for part, term in zip(self.parts, kept):
+                    pown[k, :, part * 256 : (part + 1) * 256] = term
                 self.across(k).start()
-                for part in self.parts:
-                    pown[k, :, part * 256 : (part + 1) * 256] = self.product(k, False, part)
                 if k == 1:
                     self.across(0).wait_recv()
                     self.paired(0, top, fbuf)
@@ -731,7 +750,11 @@
             for p in range(2):
                 slot()
                 net.group(unit, p, i)
-                project(layer, p, i)
+                if not layer:
+                    project(layer, p, i)
+        if layer:
+            for p in range(2):
+                project_all(layer, p)
         mix(layer, scales)
         if layer + 1 < layers:
             net.all(unit + 1)

time: 166 us -> 166 us (level)
  no operation moved by 1% of the time
where the time goes in v8:
time: 166 us
  Pallas kernels  164 us (99%)
  local copies, waits for them, and re-layouts  1.99 us (1%)
    pallas_call x1, Pallas kernels, whole_call(): pl.pallas_call(functools.partial(whole_kernel, layers, n_sp, n_tp, float(...  164 us

profile of v8, /device:TPU:1, one launch (start us, length us, event | category | flops | bytes accessed | tf_op | source)
XLA Modules:
  0.0 165.6 jit_solution(6237938867327471154)
XLA Ops:
  0.0 163.6 %both_layers.1 = bf16[512,512]{1,0:T(8,128)(2,1)} custom-call(bf16[512,512]{1,0:T(8,128)(2,1)} %stream_hbm.1, f32[2,4096]{1,0:T(2,128)} %gain_hbm.1, bf16[2,256,512]{2,1,0:T(8,128)(2,1)} %wv_hbm.1, bf16[2,256,512]{2,1,0:T(8,128)(2,1)} %wg_hbm.1, bf16[2,256,512]{2,1,0:T(8,128)(2,1)} %wo_hbm.1, f32[2,4,4096]{2,1,0:T(4,128)} %taps_hbm.1, ...), custom_call_target="tpu_custom_call" | custom-call | flops 20000000000 | bytes 8000000 | tf_op jit(solution)/shard_map/both_layers/pallas_call | solution.py:789
  163.6 2.0 %copy.9 = bf16[8,64,512]{2,1,0:T(8,128)(2,1)} copy(bf16[8,64,512]{2,0,1:T(8,128)(2,1)} %bitcast.5) | data formatting | bytes 1048576 | tf_op jit(solution)/shard_map/transpose | solution.py:864
